TPU v7x, 32 devices: a whole 2x2x4 slice. The times are simulated.
32 devices in a mesh: dp: 4 (over y, x), kv: 4 (over z), tp: 2 (over core).
Axes of the slice: x: 2, y: 2, z: 4, core: 2. Of those that a mesh axis runs over, the one named last changes fastest.
Arguments:
- tokens: bfloat16 [4, 3072, 2048], P('dp', 'kv'), may hold values from -60 to 60
- query_weight: bfloat16 [2048, 1024], P(None, 'tp'), may hold values from -0.125 to 0.125
- key_weight: bfloat16 [2048, 256], P(None, 'tp'), may hold values from -0.125 to 0.125
- value_weight: bfloat16 [2048, 256], P(None, 'tp'), may hold values from -0.125 to 0.125
- out_weight: bfloat16 [1024, 2048], P('tp'), may hold values from -3 to 3
- norm_gain: float32 [2048], P('tp'), may hold values from 0.1 to 1.9
- chosen_owner: int32 [4, 24, 4], P('dp'), may hold values from -1 to 3, as said below
- chosen_part: int32 [4, 24, 4], P('dp'), may hold values from 0 to 11, as said below
Outputs:
- attended: bfloat16 [4, 3072, 2048], P('dp', 'kv', 'tp')
Inputs may be any that keep to these rules, and one draw needn't show every extreme that they name: `chosen_owner`: within a row the indices other than -1 are different. Every named key block lies wholly before its query block's first position. Among the 6 rows of one index of kv, no index is named by more than 6 rows. `chosen_part`: 0 where the owner is -1.
All inputs are finite; a program needn't handle non-finite values.
Results may differ from a plain program's by a relative error of at most 0.014.
The roundings to bfloat16 on the way count: a program that leaves them out, or rounds other values in their place, can miss the bound.
Values may be sent and summed in bfloat16 or wider, within the bound.
A program may use at most 128 MiB of HBM per device.

v0:
```python
import functools

import jax
import jax.numpy as jnp
import numpy as np
from jax import lax
from jax.experimental import pallas as pl
from jax.experimental.pallas import tpu as pltpu
from jax.sharding import PartitionSpec as P

HEAD_DIM = 64
QUERY_BLOCK = 128
KEY_BLOCK = 64
LANES = 128
ROWS = 256
COLS = 256

rope_base = 10000.0
norm_eps = 1e-06
MESH = pl.DeviceIdType.MESH


def turn(u, cosine, sine):
    lane = lax.broadcasted_iota(jnp.int32, u.shape, 1)
    half = HEAD_DIM // 2
    swapped = jnp.where(
        lane % HEAD_DIM < half, pltpu.roll(u, LANES - half, 1), pltpu.roll(u, half, 1)
    )
    return u * cosine + swapped * sine


def spread(pair, head):
    wide = pair.astype(jnp.float32)
    swapped = pltpu.roll(wide, HEAD_DIM, 1)
    low = lax.broadcasted_iota(jnp.int32, wide.shape, 1) < HEAD_DIM
    in_low, in_high = (wide, swapped) if head == 0 else (swapped, wide)
    return jnp.concatenate(
        [jnp.where(low, in_low, 0.0), jnp.where(low, 0.0, in_high)], axis=0
    ).astype(jnp.bfloat16)


def kernel(
    devices, ids_ref, tok_hbm, wq_hbm, wk_hbm, wv_hbm, ow_hbm, gain, far_cos, far_sin, near_cos, near_sin, out,
    cosine, sine,
    tok, wq, wkv, ow, tok_sems, weight_sems,
    kv, send, pool, queries, mix, mix_other, ow_other, proj, ss, ss_other,
    kv_send, kv_recv, ow_sems, mix_send, mix_recv, ss_sems,
):
    me = lax.axis_index("kv")
    core = lax.axis_index("tp")
    other = 1 - core
    tokens = tok.shape[0]
    qblocks = tokens // QUERY_BLOCK
    chosen = ids_ref.shape[1]
    held = tokens // KEY_BLOCK
    half = ow_other.shape[1]
    row_steps = tokens // ROWS
    per_q = QUERY_BLOCK // KEY_BLOCK

    key_width = wk_hbm.shape[1]

    def tok_copy(r):
        rows = pl.ds(pl.multiple_of(r * ROWS, ROWS), ROWS)
        return pltpu.make_async_copy(tok_hbm.at[rows], tok.at[rows], tok_sems.at[r])

    wk_copy = pltpu.make_async_copy(wk_hbm, wkv.at[:, pl.ds(0, key_width)], weight_sems.at[0])
    wv_copy = pltpu.make_async_copy(
        wv_hbm, wkv.at[:, pl.ds(key_width, key_width)], weight_sems.at[1]
    )
    wq_copy = pltpu.make_async_copy(wq_hbm, wq, weight_sems.at[2])
    ow_load = pltpu.make_async_copy(ow_hbm, ow, weight_sems.at[3])
    wk_copy.start()
    wv_copy.start()
    for r in range(row_steps):
        tok_copy(r).start()
    wq_copy.start()
    ow_load.start()

    barrier = pltpu.get_barrier_semaphore()

    @pl.loop(0, devices)
    def _(j):
        @pl.when(j != me)
        def _():
            pl.semaphore_signal(barrier, inc=1, device_id={"kv": j}, device_id_type=MESH)

    pl.semaphore_signal(barrier, inc=1, device_id={"tp": other}, device_id_type=MESH)

    @pl.loop(0, qblocks)
    def _(b):
        rows = pl.ds(pl.multiple_of(b * QUERY_BLOCK, QUERY_BLOCK), QUERY_BLOCK)
        cosine[rows, :] = far_cos[b] * near_cos[...] - far_sin[b] * near_sin[...]
        sine[rows, :] = far_sin[b] * near_cos[...] + far_cos[b] * near_sin[...]

    wk_copy.wait()
    wv_copy.wait()

    @pl.loop(0, row_steps)
    def _(r):
        tok_copy(r).wait()
        rows = pl.ds(pl.multiple_of(r * ROWS, ROWS), ROWS)
        both = jnp.dot(
            tok[rows, :],
            wkv[...],
            preferred_element_type=jnp.float32,
        )
        keys = turn(both[:, :LANES], cosine[rows, :], sine[rows, :])
        joined = jnp.concatenate([keys, both[:, LANES:]], axis=1).astype(jnp.bfloat16)
        blocks = ROWS // KEY_BLOCK
        kv[pl.ds(r * blocks, blocks)] = joined.reshape(blocks, KEY_BLOCK, 2 * LANES)

    pl.semaphore_wait(barrier, devices)

    def place(src, row, s):
        at = ids_ref[row, s] - src * held
        return jnp.logical_and(at >= 0, at < held), at

    def wanted(dst, q):
        found = [place(me, dst * qblocks + q, s) for s in range(chosen)]
        return sum(jnp.where(here, at, 0) for here, at in found)

    def kv_copy(src, dst, to, q):
        return pltpu.make_async_remote_copy(
            src_ref=send.at[pl.ds(q * devices + dst, 1)],
            dst_ref=pool.at[pl.ds(q * devices + src, 1)],
            send_sem=kv_send.at[q, dst],
            recv_sem=kv_recv.at[q, src],
            device_id={"kv": to},
            device_id_type=MESH,
        )

    @pl.loop(0, qblocks)
    def _(q):
        @pl.loop(0, devices)
        def _(dst):
            @pl.when(dst > me)
            def _():
                send[pl.ds(q * devices + dst, 1)] = kv[pl.ds(wanted(dst, q), 1)]
                kv_copy(me, dst, dst, q).start()

            @pl.when(dst == me)
            def _():
                pool[pl.ds(q * devices + me, 1)] = kv[pl.ds(wanted(me, q), 1)]

            @pl.when(dst > me)
            def _():
                pool[pl.ds(q * devices + dst, 1)] = jnp.zeros(
                    (1, KEY_BLOCK, 2 * LANES), jnp.bfloat16
                )

    ow_copy = pltpu.make_async_remote_copy(
        src_ref=ow.at[:, pl.ds(pl.multiple_of(other * half, half), half)],
        dst_ref=ow_other,
        send_sem=ow_sems.at[0],
        recv_sem=ow_sems.at[1],
        device_id={"tp": other},
        device_id_type=MESH,
    )
    ow_load.wait()
    ow_copy.start()
    wq_copy.wait()

    @pl.loop(0, row_steps)
    def _(r):
        rows = pl.ds(pl.multiple_of(r * ROWS, ROWS), ROWS)
        for c in range(wq.shape[1] // COLS):
            part = jnp.dot(
                tok[rows, :], wq[:, c * COLS : (c + 1) * COLS], preferred_element_type=jnp.float32
            )
            for k in range(COLS // LANES):
                at = c * COLS + k * LANES
                queries[rows, at : at + LANES] = turn(
                    part[:, k * LANES : (k + 1) * LANES], cosine[rows, :], sine[rows, :]
                ).astype(jnp.bfloat16)

    kv_heads = key_width // HEAD_DIM
    slices = wq.shape[1] // LANES // kv_heads
    key_count = devices * KEY_BLOCK + QUERY_BLOCK

    def mix_copy(b):
        rows = pl.ds(pl.multiple_of(b * QUERY_BLOCK, QUERY_BLOCK), QUERY_BLOCK)
        return pltpu.make_async_remote_copy(
            src_ref=mix.at[rows],
            dst_ref=mix_other.at[rows],
            send_sem=mix_send.at[b],
            recv_sem=mix_recv.at[b],
            device_id={"tp": other},
            device_id_type=MESH,
        )

    def attend(b):
        row = me * qblocks + b

        @pl.loop(0, devices)
        def _(src):
            @pl.when(src < me)
            def _():
                kv_copy(src, src, src, b).wait_recv()

        rows = pl.ds(pl.multiple_of(b * QUERY_BLOCK, QUERY_BLOCK), QUERY_BLOCK)
        pieces = [pool[pl.ds(b * devices, devices)].reshape(devices * KEY_BLOCK, 2 * LANES)]
        lane = lax.broadcasted_iota(jnp.int32, (1, devices * KEY_BLOCK), 1) // KEY_BLOCK
        far = jnp.full((1, devices * KEY_BLOCK), -jnp.inf, jnp.float32)
        for src in range(devices):
            named = sum(jnp.where(place(src, row, s)[0], 1, 0) for s in range(chosen))
            far = jnp.where(lane == src, jnp.where(named > 0, 0.0, -jnp.inf), far)
        pieces.append(kv[pl.ds(b * per_q, per_q)].reshape(QUERY_BLOCK, 2 * LANES))
        near = jnp.where(
            lax.broadcasted_iota(jnp.int32, (slices * QUERY_BLOCK, QUERY_BLOCK), 0) % QUERY_BLOCK
            >= lax.broadcasted_iota(jnp.int32, (slices * QUERY_BLOCK, QUERY_BLOCK), 1),
            0.0,
            -jnp.inf,
        )
        bias = jnp.concatenate(
            [jnp.broadcast_to(far, (slices * QUERY_BLOCK, devices * KEY_BLOCK)), near], axis=1
        )
        both = jnp.concatenate(pieces, axis=0)
        for n in range(kv_heads):
            q = jnp.concatenate(
                [
                    queries[rows, (n * slices + m) * LANES : (n * slices + m + 1) * LANES]
                    for m in range(slices)
                ],
                axis=0,
            )
            scores = lax.dot_general(
                q,
                spread(both[:, :LANES], n),
                (((1,), (1,)), ((), ())),
                preferred_element_type=jnp.float32,
            )
            probs = []
            for side in range(2):
                s = scores[:, side * key_count : (side + 1) * key_count] * HEAD_DIM**-0.5 + bias
                e = jnp.exp(s - jnp.max(s, axis=1, keepdims=True))
                probs.append((e * (1.0 / jnp.sum(e, axis=1, keepdims=True))).astype(jnp.bfloat16))
            mixed = jnp.dot(
                jnp.concatenate(probs, axis=1),
                spread(both[:, LANES:], n),
                preferred_element_type=jnp.float32,
            ).astype(jnp.bfloat16)
            for m in range(slices):
                at = (n * slices + m) * LANES
                mix[rows, at : at + LANES] = mixed[m * QUERY_BLOCK : (m + 1) * QUERY_BLOCK]
        mix_copy(b).start()

    blocks_in = ROWS // QUERY_BLOCK

    def project(r):
        for k in range(blocks_in):
            mix_copy(r * blocks_in + k).wait_recv()
        rows = pl.ds(pl.multiple_of(r * ROWS, ROWS), ROWS)
        total = jnp.zeros((ROWS, LANES), jnp.float32)
        for c in range(half // COLS):
            mine = jnp.dot(
                mix[rows, :],
                ow[:, pl.ds(pl.multiple_of(core * half + c * COLS, COLS), COLS)],
                preferred_element_type=jnp.float32,
            ).astype(jnp.bfloat16)
            theirs = jnp.dot(
                mix_other[rows, :],
                ow_other[:, c * COLS : (c + 1) * COLS],
                preferred_element_type=jnp.float32,
            ).astype(jnp.bfloat16)
            added = mine.astype(jnp.float32) + theirs.astype(jnp.float32)
            proj[rows, c * COLS : (c + 1) * COLS] = added
            for k in range(COLS // LANES):
                piece = added[:, k * LANES : (k + 1) * LANES]
                total = total + piece * piece
        for k in range(ROWS // LANES):
            ss[r * (ROWS // LANES) + k] = jnp.sum(
                total[k * LANES : (k + 1) * LANES].T, axis=0, keepdims=True
            )

    ow_copy.wait_recv()

    @pl.loop(0, row_steps)
    def _(r):
        @pl.loop(0, blocks_in)
        def _(k):
            attend(r * blocks_in + k)

        @pl.when(r > 0)
        def _():
            project(r - 1)

    project(row_steps - 1)

    ss_copy = pltpu.make_async_remote_copy(
        src_ref=ss,
        dst_ref=ss_other,
        send_sem=ss_sems.at[0],
        recv_sem=ss_sems.at[1],
        device_id={"tp": other},
        device_id_type=MESH,
    )
    ss_copy.start()

    @pl.loop(0, qblocks)
    def _(q):
        @pl.loop(0, devices)
        def _(dst):
            @pl.when(dst > me)
            def _():
                kv_copy(me, dst, dst, q).wait_send()

    ow_copy.wait_send()

    @pl.loop(0, qblocks)
    def _(b):
        mix_copy(b).wait_send()

    ss_copy.wait()

    @pl.loop(0, qblocks)
    def _(b):
        rows = pl.ds(pl.multiple_of(b * LANES, LANES), LANES)
        scale = lax.rsqrt((ss[b] + ss_other[b]) / (2 * half) + norm_eps)
        scale = jnp.broadcast_to(scale, (LANES, LANES)).T
        for c in range(half // LANES):
            at = slice(c * LANES, (c + 1) * LANES)
            out[rows, at] = (proj[rows, at] * scale * gain[:, at]).astype(jnp.bfloat16)


def body(
    tokens, query_weight, key_weight, value_weight, out_weight, norm_gain, chosen_owner, chosen_part
):
    row_data = tokens[0]
    count = row_data.shape[0]
    devices = lax.axis_size("kv")
    qblocks = count // QUERY_BLOCK
    half_dim = HEAD_DIM // 2
    lane = np.arange(LANES)
    frequency = (rope_base ** (-(lane % half_dim) / half_dim)).astype(np.float32)
    sign = np.where(lane % HEAD_DIM < half_dim, -1.0, 1.0).astype(np.float32)
    inner = np.arange(QUERY_BLOCK)[:, None] * frequency.astype(np.float64)
    near_cos = np.cos(inner).astype(np.float32)
    near_sin = (sign * np.sin(inner)).astype(np.float32)
    starts = lax.axis_index("kv") * count + QUERY_BLOCK * jnp.arange(qblocks, dtype=jnp.int32)
    angles = starts.astype(jnp.float32)[:, None, None] * frequency
    far_cos, far_sin = jnp.cos(angles), sign * jnp.sin(angles)
    ids = jnp.where(
        chosen_owner[0] >= 0, chosen_owner[0] * (count // KEY_BLOCK) + chosen_part[0], -1
    )
    heads_width = query_weight.shape[1]
    half = norm_gain.shape[0]
    vmem = pl.BlockSpec(memory_space=pltpu.VMEM)
    smem = pl.BlockSpec(memory_space=pltpu.SMEM)
    bf16, f32 = jnp.bfloat16, jnp.float32
    result = pl.pallas_call(
        functools.partial(kernel, devices),
        out_shape=jax.ShapeDtypeStruct((count, half), bf16),
        in_specs=[smem] + [pl.BlockSpec(memory_space=pl.ANY)] * 5 + [vmem] * 5,
        out_specs=vmem,
        scratch_shapes=[
            pltpu.VMEM((count, LANES), f32),
            pltpu.VMEM((count, LANES), f32),
            pltpu.VMEM(row_data.shape, bf16),
            pltpu.VMEM(query_weight.shape, bf16),
            pltpu.VMEM((key_weight.shape[0], 2 * key_weight.shape[1]), bf16),
            pltpu.VMEM(out_weight.shape, bf16),
            pltpu.SemaphoreType.DMA((count // ROWS,)),
            pltpu.SemaphoreType.DMA((4,)),
            pltpu.VMEM((count // KEY_BLOCK, KEY_BLOCK, 2 * LANES), bf16),
            pltpu.VMEM((devices * qblocks, KEY_BLOCK, 2 * LANES), bf16),
            pltpu.VMEM((devices * qblocks, KEY_BLOCK, 2 * LANES), bf16),
            pltpu.VMEM((count, heads_width), bf16),
            pltpu.VMEM((count, heads_width), bf16),
            pltpu.VMEM((count, heads_width), bf16),
            pltpu.VMEM((out_weight.shape[0], half), bf16),
            pltpu.VMEM((count, half), f32),
            pltpu.VMEM((qblocks, 1, LANES), f32),
            pltpu.VMEM((qblocks, 1, LANES), f32),
            pltpu.SemaphoreType.DMA((qblocks, devices)),
            pltpu.SemaphoreType.DMA((qblocks, devices)),
            pltpu.SemaphoreType.DMA((2,)),
            pltpu.SemaphoreType.DMA((qblocks,)),
            pltpu.SemaphoreType.DMA((qblocks,)),
            pltpu.SemaphoreType.DMA((2,)),
        ],
        compiler_params=pltpu.CompilerParams(
            collective_id=0, has_side_effects=True, vmem_limit_bytes=60 * 1024 * 1024
        ),
    )(
        ids, row_data, query_weight, key_weight, value_weight,
        out_weight, norm_gain[None], far_cos, far_sin,
        jnp.asarray(near_cos), jnp.asarray(near_sin),
    )
    return result[None]


def solution(mesh):
    placed = (
        P("dp", "kv", None),
        P(None, "tp"),
        P(None, "tp"),
        P(None, "tp"),
        P("tp", None),
        P("tp"),
        P("dp", None, None),
        P("dp", None, None),
    )
    return jax.shard_map(
        body, mesh=mesh, in_specs=placed, out_specs=P("dp", "kv", "tp"), check_vma=False
    )
```

profile of v0, /device:TPU:27, one launch (start us, length us, event | category | flops | bytes accessed | tf_op | source)
XLA Modules:
  0.0 35.8 jit_solution(9237270610033573965)
XLA Ops:
  0.0 0.7 %select_bitcast_fusion = s32[24,4]{0,1:T(4,128)S(1)} fusion(s32[1,24,4]{1,2,0:T(4,128)} %param.19, s32[1,24,4]{1,2,0:T(4,128)} %param.18), kind=kLoop, calls=%fused_computation.3 | loop fusion | flops 384 | bytes 1152 | tf_op jit(solution)/shard_map/jit(_where)/select_n | solution.py:342
  0.7 1.4 %fusion = (f32[6,1,128]{2,1,0:T(1,128)}, f32[6,1,128]{2,1,0:T(1,128)}) fusion(f32[128]{0:T(128)} %constant.25.clone, f32[128]{0:T(128)} %constant.24.clone, f32[6]{0:T(128)S(1)} %add_convert_fusion), kind=kLoop, calls=%fused_computation.2 | loop fusion | flops 1536 | bytes 7192 | tf_op jit(solution)/shard_map/mul | solution.py:341
  2.1 0.7 %copy.13.ids_ref = s32[24,4]{1,0:T(8,128)} copy(s32[24,4]{0,1:T(4,128)S(1)} %select_bitcast_fusion) | data formatting | bytes 768 | tf_op jit(solution)/shard_map/jit(_where)/select_n | solution.py:342
  2.8 30.3 %shard_map.118 = bf16[768,1024]{1,0:T(8,128)(2,1)} custom-call(s32[24,4]{1,0:T(8,128)} %copy.13.ids_ref, bf16[768,2048]{1,0:T(8,128)(2,1)} %bitcast.6, bf16[2048,512]{1,0:T(8,128)(2,1)} %wq_hbm.1, bf16[2048,128]{1,0:T(8,128)(2,1)} %wk_hbm.1, bf16[2048,128]{1,0:T(8,128)(2,1)} %wv_hbm.1, bf16[512,2048]{1,0:T(8,128)(2,1)} %ow_hbm.1, f32[1,1024]{1,0:T(1,128)} %bitcast.7, ...), custom_call_target="tpu_custom_call" | custom-call | tf_op jit(solution)/shard_map/pallas_call | solution.py:350
  33.1 2.7 %copy.15 = bf16[1,768,1024]{2,1,0:T(8,128)(2,1)} copy(bf16[1,768,1024]{2,1,0:T(8,128)(2,1)} %bitcast.5) | data formatting | bytes 3145728
  (1 shorter events, 0.0 us)
where the time goes:
time: 36 us; the launch traced here: 35.8 us
  Pallas kernels  30.3 us (84%)
  local copies, waits for them, and re-layouts  3.35 us (9%)
  other arithmetic  2.14 us (6%)
    pallas_call x1, Pallas kernels, body(): pl.pallas_call(functools.partial(kernel, devices), out_shape=jax.ShapeDty...  30.3 us
    unnamed x1, local copies, waits for them, and re-layouts  2.67 us
    mul x1, other arithmetic, body(): far_cos, far_sin = (jnp.cos(angles), sign * jnp.sin(angles))  1.43 us

commit v1 on v0

--- a/solution.py
+++ b/solution.py
@@ -40,8 +40,8 @@
 
 
 def kernel(
-    devices, ids_ref, tok_hbm, wq_hbm, wk_hbm, wv_hbm, ow_hbm, gain, far_cos, far_sin, near_cos, near_sin, out,
-    cosine, sine,
+    devices, owner_hbm, part_hbm, tok_hbm, wq_hbm, wk_hbm, wv_hbm, ow_hbm, gain_hbm, trig_hbm, out,
+    owner_ref, part_ref, gain, trig, small_sems, cosine, sine,
     tok, wq, wkv, ow, tok_sems, weight_sems,
     kv, send, pool, queries, mix, mix_other, ow_other, proj, ss, ss_other,
     kv_send, kv_recv, ow_sems, mix_send, mix_recv, ss_sems,
@@ -51,8 +51,7 @@
     other = 1 - core
     tokens = tok.shape[0]
     qblocks = tokens // QUERY_BLOCK
-    chosen = ids_ref.shape[1]
-    held = tokens // KEY_BLOCK
+    chosen = owner_ref.shape[0]
     half = ow_other.shape[1]
     row_steps = tokens // ROWS
     per_q = QUERY_BLOCK // KEY_BLOCK
@@ -69,10 +68,19 @@
     )
     wq_copy = pltpu.make_async_copy(wq_hbm, wq, weight_sems.at[2])
     ow_load = pltpu.make_async_copy(ow_hbm, ow, weight_sems.at[3])
+    small = [
+        pltpu.make_async_copy(trig_hbm, trig, small_sems.at[0]),
+        pltpu.make_async_copy(owner_hbm, owner_ref, small_sems.at[1]),
+        pltpu.make_async_copy(part_hbm, part_ref, small_sems.at[2]),
+        pltpu.make_async_copy(gain_hbm, gain, small_sems.at[3]),
+    ]
+    small[0].start()
     wk_copy.start()
     wv_copy.start()
     for r in range(row_steps):
         tok_copy(r).start()
+    for copy in small[1:]:
+        copy.start()
     wq_copy.start()
     ow_load.start()
 
@@ -86,11 +94,18 @@
 
     pl.semaphore_signal(barrier, inc=1, device_id={"tp": other}, device_id_type=MESH)
 
+    small[0].wait()
+    near_cos = trig[0:QUERY_BLOCK, :]
+    near_sin = trig[QUERY_BLOCK : 2 * QUERY_BLOCK, :]
+
     @pl.loop(0, qblocks)
     def _(b):
         rows = pl.ds(pl.multiple_of(b * QUERY_BLOCK, QUERY_BLOCK), QUERY_BLOCK)
-        cosine[rows, :] = far_cos[b] * near_cos[...] - far_sin[b] * near_sin[...]
-        sine[rows, :] = far_sin[b] * near_cos[...] + far_cos[b] * near_sin[...]
+        at = 2 * QUERY_BLOCK + me * qblocks + b
+        far_cos = trig[pl.ds(at, 1), :]
+        far_sin = trig[pl.ds(at + devices * qblocks, 1), :]
+        cosine[rows, :] = far_cos * near_cos - far_sin * near_sin
+        sine[rows, :] = far_sin * near_cos + far_cos * near_sin
 
     wk_copy.wait()
     wv_copy.wait()
@@ -112,8 +127,7 @@
     pl.semaphore_wait(barrier, devices)
 
     def place(src, row, s):
-        at = ids_ref[row, s] - src * held
-        return jnp.logical_and(at >= 0, at < held), at
+        return owner_ref[s, row] == src, part_ref[s, row]
 
     def wanted(dst, q):
         found = [place(me, dst * qblocks + q, s) for s in range(chosen)]
@@ -128,6 +142,9 @@
             device_id={"kv": to},
             device_id_type=MESH,
         )
+
+    for copy in small[1:]:
+        copy.wait()
 
     @pl.loop(0, qblocks)
     def _(q):
@@ -322,6 +339,28 @@
             out[rows, at] = (proj[rows, at] * scale * gain[:, at]).astype(jnp.bfloat16)
 
 
+def store_kernel(held, out, sems):
+    def copy(b):
+        rows = pl.ds(b * QUERY_BLOCK, QUERY_BLOCK)
+        return pltpu.make_async_copy(held.at[rows], out.at[rows], sems.at[b])
+
+    for b in range(sems.shape[0]):
+        copy(b).start()
+    for b in range(sems.shape[0]):
+        copy(b).wait()
+
+
+def trig_table(blocks):
+    half_dim = HEAD_DIM // 2
+    lane = np.arange(LANES)
+    frequency = (rope_base ** (-(lane % half_dim) / half_dim)).astype(np.float32)
+    sign = np.where(lane % HEAD_DIM < half_dim, -1.0, 1.0)
+    near = np.arange(QUERY_BLOCK)[:, None] * frequency.astype(np.float64)
+    far = (np.arange(blocks)[:, None] * np.float32(QUERY_BLOCK) * frequency).astype(np.float64)
+    parts = [np.cos(near), sign * np.sin(near), np.cos(far), sign * np.sin(far)]
+    return np.concatenate(parts, axis=0).astype(np.float32)
+
+
 def body(
     tokens, query_weight, key_weight, value_weight, out_weight, norm_gain, chosen_owner, chosen_part
 ):
@@ -329,30 +368,29 @@
     count = row_data.shape[0]
     devices = lax.axis_size("kv")
     qblocks = count // QUERY_BLOCK
-    half_dim = HEAD_DIM // 2
-    lane = np.arange(LANES)
-    frequency = (rope_base ** (-(lane % half_dim) / half_dim)).astype(np.float32)
-    sign = np.where(lane % HEAD_DIM < half_dim, -1.0, 1.0).astype(np.float32)
-    inner = np.arange(QUERY_BLOCK)[:, None] * frequency.astype(np.float64)
-    near_cos = np.cos(inner).astype(np.float32)
-    near_sin = (sign * np.sin(inner)).astype(np.float32)
-    starts = lax.axis_index("kv") * count + QUERY_BLOCK * jnp.arange(qblocks, dtype=jnp.int32)
-    angles = starts.astype(jnp.float32)[:, None, None] * frequency
-    far_cos, far_sin = jnp.cos(angles), sign * jnp.sin(angles)
-    ids = jnp.where(
-        chosen_owner[0] >= 0, chosen_owner[0] * (count // KEY_BLOCK) + chosen_part[0], -1
-    )
     heads_width = query_weight.shape[1]
     half = norm_gain.shape[0]
+    hbm = pl.BlockSpec(memory_space=pl.ANY)
     vmem = pl.BlockSpec(memory_space=pltpu.VMEM)
-    smem = pl.BlockSpec(memory_space=pltpu.SMEM)
     bf16, f32 = jnp.bfloat16, jnp.float32
+    slots = chosen_owner.shape[1:][::-1]
+    trig = trig_table(devices * qblocks)
+    operands = [
+        chosen_owner[0].T, chosen_part[0].T, row_data, query_weight, key_weight, value_weight,
+        out_weight, norm_gain[None], jnp.asarray(trig),
+    ]
+    operands = [pltpu.with_memory_space_constraint(x, pltpu.HBM) for x in operands]
     result = pl.pallas_call(
         functools.partial(kernel, devices),
-        out_shape=jax.ShapeDtypeStruct((count, half), bf16),
-        in_specs=[smem] + [pl.BlockSpec(memory_space=pl.ANY)] * 5 + [vmem] * 5,
+        out_shape=pltpu.VMEM((count, half), bf16),
+        in_specs=[hbm] * len(operands),
         out_specs=vmem,
         scratch_shapes=[
+            pltpu.SMEM(slots, jnp.int32),
+            pltpu.SMEM(slots, jnp.int32),
+            pltpu.VMEM((1, half), f32),
+            pltpu.VMEM(trig.shape, f32),
+            pltpu.SemaphoreType.DMA((4,)),
             pltpu.VMEM((count, LANES), f32),
             pltpu.VMEM((count, LANES), f32),
             pltpu.VMEM(row_data.shape, bf16),
@@ -379,14 +417,17 @@
             pltpu.SemaphoreType.DMA((2,)),
         ],
         compiler_params=pltpu.CompilerParams(
-            collective_id=0, has_side_effects=True, vmem_limit_bytes=60 * 1024 * 1024
+            collective_id=0, has_side_effects=True, vmem_limit_bytes=48 * 1024 * 1024
         ),
-    )(
-        ids, row_data, query_weight, key_weight, value_weight,
-        out_weight, norm_gain[None], far_cos, far_sin,
-        jnp.asarray(near_cos), jnp.asarray(near_sin),
-    )
-    return result[None]
+    )(*operands)
+    return pl.pallas_call(
+        store_kernel,
+        out_shape=jax.ShapeDtypeStruct((count, half), bf16),
+        in_specs=[vmem],
+        out_specs=hbm,
+        scratch_shapes=[pltpu.SemaphoreType.DMA((qblocks,))],
+        compiler_params=pltpu.CompilerParams(vmem_limit_bytes=4 * 1024 * 1024),
+    )(pltpu.with_memory_space_constraint(result, pltpu.VMEM))[None]
 
 
 def solution(mesh):

time: 36 us -> 29.7 us (0.82)
  the two profiles are of different devices: /device:TPU:27 before, /device:TPU:29 now
where the time goes in v1:
time: 29.7 us; the launch traced here: 29.6 us
  Pallas kernels  29.6 us (100%)
    pallas_call x1, Pallas kernels, body(): pl.pallas_call(functools.partial(kernel, devices), out_shape=pltpu.VMEM((...  28.4 us
    pallas_call x1, Pallas kernels, body(): pl.pallas_call(store_kernel, out_shape=jax.ShapeDtypeStruct((count, half)...  1.19 us

profile of v1, /device:TPU:29, one launch (start us, length us, event | category | flops | bytes accessed | tf_op | source)
XLA Modules:
  0.0 29.6 jit_solution(10776796987595868569)
XLA Ops:
  0.0 28.4 %shard_map.91.held = bf16[768,1024]{1,0:T(8,128)(2,1)S(1)} custom-call(s32[4,24]{1,0:T(4,128)} %bitcast.11, s32[4,24]{1,0:T(4,128)} %bitcast.12, bf16[768,2048]{1,0:T(8,128)(2,1)} %bitcast.9, bf16[2048,512]{1,0:T(8,128)(2,1)} %wq_hbm.1, bf16[2048,128]{1,0:T(8,128)(2,1)} %wk_hbm.1, bf16[2048,128]{1,0:T(8,128)(2,1)} %wv_hbm.1, bf16[512,2048]{1,0:T(8,128)(2,1)} %ow_hbm.1, ...), custom_call_target="tpu_custom_call" | custom-call | tf_op jit(solution)/shard_map/pallas_call | solution.py:383
  28.4 1.2 %shard_map.92 = bf16[768,1024]{1,0:T(8,128)(2,1)} custom-call(bf16[768,1024]{1,0:T(8,128)(2,1)S(1)} %shard_map.91.held), custom_call_target="tpu_custom_call" | custom-call | tf_op jit(solution)/shard_map/pallas_call | solution.py:423

commit v2 on v1

v2 whole, which is shorter than its diff:
```python
import functools

import jax
import jax.numpy as jnp
import numpy as np
from jax import lax
from jax.experimental import pallas as pl
from jax.experimental.pallas import tpu as pltpu
from jax.sharding import PartitionSpec as P

HEAD_DIM = 64
QUERY_BLOCK = 128
KEY_BLOCK = 64
LANES = 128
ROWS = 256
COLS = 256

rope_base = 10000.0
norm_eps = 1e-06
hidden = -1e38
MESH = pl.DeviceIdType.MESH


def low_lanes(shape):
    return lax.broadcasted_iota(jnp.int32, shape, 1) < HEAD_DIM


def turn(u, cosine, sine):
    lane = lax.broadcasted_iota(jnp.int32, u.shape, 1)
    half = HEAD_DIM // 2
    swapped = jnp.where(
        lane % HEAD_DIM < half, pltpu.roll(u, LANES - half, 1), pltpu.roll(u, half, 1)
    )
    return u * cosine + swapped * sine


def kernel(
    devices, owner_hbm, part_hbm, tok_hbm, wq_hbm, wk_hbm, wv_hbm, ow_hbm, gain_hbm, trig_hbm, out,
    owner_ref, part_ref, gain, trig, small_sems, cosine, sine, eye, causal,
    tok, wq, wkv, ow, tok_sems, weight_sems, ow_load_sems,
    kv, send, pool, queries, mix, mix_other, ow_other, partial, proj,
    kv_send, kv_recv, ow_sems, mix_send, mix_recv,
):
    me = lax.axis_index("kv")
    core = lax.axis_index("tp")
    other = 1 - core
    tokens = tok.shape[0]
    qblocks = tokens // QUERY_BLOCK
    chosen = owner_ref.shape[0]
    half = gain.shape[1]
    row_steps = tokens // ROWS
    per_q = QUERY_BLOCK // KEY_BLOCK
    key_width = wk_hbm.shape[1]
    slices = wq.shape[1] // LANES
    heads = wq.shape[1] // HEAD_DIM
    bf16, f32 = jnp.bfloat16, jnp.float32

    def tok_copy(r):
        rows = pl.ds(pl.multiple_of(r * ROWS, ROWS), ROWS)
        return pltpu.make_async_copy(tok_hbm.at[rows], tok.at[rows], tok_sems.at[r])

    wk_copy = pltpu.make_async_copy(wk_hbm, wkv.at[:, pl.ds(0, key_width)], weight_sems.at[0])
    wv_copy = pltpu.make_async_copy(
        wv_hbm, wkv.at[:, pl.ds(key_width, key_width)], weight_sems.at[1]
    )
    wq_copy = pltpu.make_async_copy(wq_hbm, wq, weight_sems.at[2])
    ow_loads = []
    for m in range(slices):
        for g in range(2):
            ow_loads.append(
                pltpu.make_async_copy(
                    ow_hbm.at[pl.ds((g * slices + m) * HEAD_DIM, HEAD_DIM)],
                    ow.at[pl.ds((2 * m + g) * HEAD_DIM, HEAD_DIM)],
                    ow_load_sems.at[2 * m + g],
                )
            )
    small = [
        pltpu.make_async_copy(trig_hbm, trig, small_sems.at[0]),
        pltpu.make_async_copy(owner_hbm, owner_ref, small_sems.at[1]),
        pltpu.make_async_copy(part_hbm, part_ref, small_sems.at[2]),
        pltpu.make_async_copy(gain_hbm, gain, small_sems.at[3]),
    ]
    small[0].start()
    wk_copy.start()
    wv_copy.start()
    for r in range(row_steps):
        tok_copy(r).start()
    for copy in small[1:]:
        copy.start()

    barrier = pltpu.get_barrier_semaphore()

    @pl.loop(0, devices)
    def _(j):
        @pl.when(j != me)
        def _():
            pl.semaphore_signal(barrier, inc=1, device_id={"kv": j}, device_id_type=MESH)

    pl.semaphore_signal(barrier, inc=1, device_id={"tp": other}, device_id_type=MESH)

    square = (QUERY_BLOCK, QUERY_BLOCK)
    first = lax.broadcasted_iota(jnp.int32, square, 0)
    second = lax.broadcasted_iota(jnp.int32, square, 1)
    eye[...] = jnp.where(first == second, 1.0, 0.0).astype(bf16)
    causal[...] = jnp.where(second >= first, 0.0, hidden).astype(bf16)

    small[0].wait()
    near_cos = trig[0:QUERY_BLOCK, :]
    near_sin = trig[QUERY_BLOCK : 2 * QUERY_BLOCK, :]

    @pl.loop(0, qblocks)
    def _(b):
        rows = pl.ds(pl.multiple_of(b * QUERY_BLOCK, QUERY_BLOCK), QUERY_BLOCK)
        at = 2 * QUERY_BLOCK + me * qblocks + b
        far_cos = trig[pl.ds(at, 1), :]
        far_sin = trig[pl.ds(at + devices * qblocks, 1), :]
        cosine[rows, :] = far_cos * near_cos - far_sin * near_sin
        sine[rows, :] = far_sin * near_cos + far_cos * near_sin

    wk_copy.wait()
    wv_copy.wait()

    @pl.loop(0, row_steps)
    def _(r):
        tok_copy(r).wait()

        @pl.when(r == 0)
        def _():
            wq_copy.start()
            for copy in ow_loads:
                copy.start()

        rows = pl.ds(pl.multiple_of(r * ROWS, ROWS), ROWS)
        both = jnp.dot(tok[rows, :], wkv[...], preferred_element_type=f32)
        keys = turn(both[:, :LANES], cosine[rows, :], sine[rows, :])
        joined = jnp.concatenate([keys, both[:, LANES:]], axis=1).astype(bf16)
        blocks = ROWS // KEY_BLOCK
        kv[pl.ds(r * blocks, blocks)] = joined.reshape(blocks, KEY_BLOCK, 2 * LANES)

    for copy in small[1:]:
        copy.wait()
    pl.semaphore_wait(barrier, devices)

    def place(src, row, s):
        return owner_ref[s, row] == src, part_ref[s, row]

    def wanted(dst, q):
        found = [place(me, dst * qblocks + q, s) for s in range(chosen)]
        return sum(jnp.where(here, at, 0) for here, at in found)

    def kv_copy(src, dst, to, q):
        return pltpu.make_async_remote_copy(
            src_ref=send.at[pl.ds(q * devices + dst, 1)],
            dst_ref=pool.at[pl.ds(q * devices + src, 1)],
            send_sem=kv_send.at[q, dst],
            recv_sem=kv_recv.at[q, src],
            device_id={"kv": to},
            device_id_type=MESH,
        )

    @pl.loop(0, qblocks)
    def _(q):
        @pl.loop(0, devices - 1)
        def _(step):
            dst = devices - 1 - step

            @pl.when(dst > me)
            def _():
                send[pl.ds(q * devices + dst, 1)] = kv[pl.ds(wanted(dst, q), 1)]
                kv_copy(me, dst, dst, q).start()

    @pl.loop(0, qblocks)
    def _(q):
        pool[pl.ds(q * devices + me, 1)] = kv[pl.ds(wanted(me, q), 1)]

        @pl.loop(0, devices)
        def _(src):
            @pl.when(src > me)
            def _():
                pool[pl.ds(q * devices + src, 1)] = jnp.zeros((1, KEY_BLOCK, 2 * LANES), bf16)

    ow_copy = pltpu.make_async_remote_copy(
        src_ref=ow,
        dst_ref=ow_other,
        send_sem=ow_sems.at[0],
        recv_sem=ow_sems.at[1],
        device_id={"tp": other},
        device_id_type=MESH,
    )
    wq_copy.wait()

    @pl.loop(0, row_steps)
    def _(r):
        @pl.when(r == 1)
        def _():
            for copy in ow_loads:
                copy.wait()
            ow_copy.start()

        rows = pl.ds(pl.multiple_of(r * ROWS, ROWS), ROWS)
        scale = HEAD_DIM**-0.5
        scaled_cos, scaled_sin = cosine[rows, :] * scale, sine[rows, :] * scale
        for c in range(wq.shape[1] // COLS):
            part = jnp.dot(
                tok[rows, :], wq[:, c * COLS : (c + 1) * COLS], preferred_element_type=f32
            )
            for k in range(COLS // LANES):
                turned = turn(part[:, k * LANES : (k + 1) * LANES], scaled_cos, scaled_sin)
                away = pltpu.roll(turned, HEAD_DIM, 1)
                for j in range(2):
                    head = 2 * (c * (COLS // LANES) + k) + j
                    group, m = head // slices, head % slices
                    lanes = slice(group * HEAD_DIM, (group + 1) * HEAD_DIM)
                    at = m * LANES + group * HEAD_DIM
                    queries[rows, at : at + HEAD_DIM] = (
                        turned if group == j else away
                    )[:, lanes].astype(bf16)

    key_count = devices * KEY_BLOCK + QUERY_BLOCK

    def mix_copy(b):
        rows = pl.ds(pl.multiple_of(b * QUERY_BLOCK, QUERY_BLOCK), QUERY_BLOCK)
        return pltpu.make_async_remote_copy(
            src_ref=mix.at[rows],
            dst_ref=mix_other.at[rows],
            send_sem=mix_send.at[b],
            recv_sem=mix_recv.at[b],
            device_id={"tp": other},
            device_id_type=MESH,
        )

    low_mask = jnp.where(low_lanes((key_count, LANES)), 1.0, 0.0).astype(bf16)
    high_mask = jnp.where(low_lanes((key_count, LANES)), 0.0, 1.0).astype(bf16)

    def attend(b):
        row = me * qblocks + b

        @pl.loop(0, devices)
        def _(src):
            @pl.when(src < me)
            def _():
                kv_copy(src, src, src, b).wait_recv()

        rows = pl.ds(pl.multiple_of(b * QUERY_BLOCK, QUERY_BLOCK), QUERY_BLOCK)
        far = pool[pl.ds(b * devices, devices)].reshape(devices * KEY_BLOCK, 2 * LANES)
        near = kv[pl.ds(b * per_q, per_q)].reshape(QUERY_BLOCK, 2 * LANES)
        both = jnp.concatenate([far, near], axis=0)
        keys, values = both[:, :LANES], both[:, LANES:]
        bias = []
        for src in range(devices):
            named = sum(jnp.where(place(src, row, s)[0], 1, 0) for s in range(chosen))
            bias.append(
                jnp.full((KEY_BLOCK, LANES), jnp.where(named > 0, 0.0, hidden), f32).astype(bf16)
            )
        bias = jnp.concatenate(bias + [causal[...]], axis=0)
        wide_keys = jnp.concatenate(
            [
                jnp.concatenate([keys * low_mask, bias], axis=1),
                jnp.concatenate([keys * high_mask, bias], axis=1),
            ],
            axis=0,
        )
        wide_values = jnp.concatenate(
            [
                jnp.concatenate([values * low_mask, low_mask], axis=1),
                jnp.concatenate([values * high_mask, high_mask], axis=1),
            ],
            axis=0,
        )
        for pair in range(0, slices, 2):
            q = jnp.concatenate(
                [
                    jnp.concatenate([queries[rows, m * LANES : (m + 1) * LANES], eye[...]], axis=1)
                    for m in (pair, pair + 1)
                ],
                axis=0,
            )
            scores = lax.dot_general(
                q, wide_keys, (((1,), (1,)), ((), ())), preferred_element_type=f32
            )
            weights = []
            for side in range(2):
                s = scores[:, side * key_count : (side + 1) * key_count]
                weights.append(jnp.exp(s - jnp.max(s, axis=1, keepdims=True)).astype(bf16))
            mixed = jnp.dot(
                jnp.concatenate(weights, axis=1), wide_values, preferred_element_type=f32
            )
            mixed = (mixed[:, :LANES] / mixed[:, LANES:]).astype(bf16)
            for k in range(2):
                at = (pair + k) * LANES
                mix[rows, at : at + LANES] = mixed[k * QUERY_BLOCK : (k + 1) * QUERY_BLOCK]
        mix_copy(b).start()

    def part_of(left, right, rows, side, c):
        cols = pl.ds(pl.multiple_of(side * half + c * COLS, COLS), COLS)
        return jnp.dot(left[rows, :], right[:, cols], preferred_element_type=f32).astype(bf16)

    def project_mine(start, count):
        rows = pl.ds(start, count)
        for n, side in enumerate((other, core)):
            for c in range(half // COLS):
                at = n * half + c * COLS
                partial[:count, at : at + COLS] = part_of(mix, ow, rows, side, c)

    def project(start, count, ready=False):
        rows = pl.ds(start, count)
        total = jnp.zeros((count, LANES), f32)
        for n, side in enumerate((other, core)):
            for c in range(half // COLS):
                at = n * half + c * COLS
                mine = partial[:count, at : at + COLS] if ready else part_of(mix, ow, rows, side, c)
                theirs = part_of(mix_other, ow_other, rows, side, c)
                added = mine.astype(f32) + theirs.astype(f32)
                if side is core:
                    proj[:count, c * COLS : (c + 1) * COLS] = added
                for k in range(COLS // LANES):
                    piece = added[:, k * LANES : (k + 1) * LANES]
                    total = total + piece * piece
        scale = lax.rsqrt(jnp.sum(total, axis=1, keepdims=True) / (2 * half) + norm_eps)
        for c in range(half // LANES):
            at = slice(c * LANES, (c + 1) * LANES)
            out[rows, at] = (proj[:count, at] * scale * gain[:, at]).astype(bf16)

    blocks_in = ROWS // QUERY_BLOCK

    @pl.loop(0, row_steps)
    def _(r):
        @pl.loop(0, blocks_in)
        def _(k):
            attend(r * blocks_in + k)

            @pl.when(jnp.logical_and(r == 1, k == 0))
            def _():
                ow_copy.wait_recv()

            @pl.when(jnp.logical_and(r > 0, k == 0))
            def _():
                for j in range(blocks_in):
                    mix_copy((r - 1) * blocks_in + j).wait_recv()
                project(pl.multiple_of((r - 1) * ROWS, ROWS), ROWS)

    for b in range(qblocks - blocks_in, qblocks - 1):
        mix_copy(b).wait_recv()
        project(b * QUERY_BLOCK, QUERY_BLOCK)
    last = qblocks - 1
    project_mine(last * QUERY_BLOCK, QUERY_BLOCK)

    @pl.loop(0, qblocks)
    def _(q):
        @pl.loop(0, devices)
        def _(dst):
            @pl.when(dst > me)
            def _():
                kv_copy(me, dst, dst, q).wait_send()

    ow_copy.wait_send()

    @pl.loop(0, last)
    def _(b):
        mix_copy(b).wait_send()

    mix_copy(last).wait_recv()
    project(last * QUERY_BLOCK, QUERY_BLOCK, ready=True)
    mix_copy(last).wait_send()


def store_kernel(held, out, sems):
    def copy(b):
        rows = pl.ds(b * QUERY_BLOCK, QUERY_BLOCK)
        return pltpu.make_async_copy(held.at[rows], out.at[rows], sems.at[b])

    for b in range(sems.shape[0]):
        copy(b).start()
    for b in range(sems.shape[0]):
        copy(b).wait()


def trig_table(blocks):
    half_dim = HEAD_DIM // 2
    lane = np.arange(LANES)
    frequency = (rope_base ** (-(lane % half_dim) / half_dim)).astype(np.float32)
    sign = np.where(lane % HEAD_DIM < half_dim, -1.0, 1.0)
    near = np.arange(QUERY_BLOCK)[:, None] * frequency.astype(np.float64)
    far = (np.arange(blocks)[:, None] * np.float32(QUERY_BLOCK) * frequency).astype(np.float64)
    parts = [np.cos(near), sign * np.sin(near), np.cos(far), sign * np.sin(far)]
    return np.concatenate(parts, axis=0).astype(np.float32)


def body(
    tokens, query_weight, key_weight, value_weight, out_weight, norm_gain, chosen_owner, chosen_part
):
    row_data = tokens[0]
    count = row_data.shape[0]
    devices = lax.axis_size("kv")
    qblocks = count // QUERY_BLOCK
    heads_width = query_weight.shape[1]
    half = norm_gain.shape[0]
    hbm = pl.BlockSpec(memory_space=pl.ANY)
    vmem = pl.BlockSpec(memory_space=pltpu.VMEM)
    bf16, f32 = jnp.bfloat16, jnp.float32
    slots = chosen_owner.shape[1:][::-1]
    trig = trig_table(devices * qblocks)
    operands = [
        chosen_owner[0].T, chosen_part[0].T, row_data, query_weight, key_weight, value_weight,
        out_weight, norm_gain[None], jnp.asarray(trig),
    ]
    operands = [pltpu.with_memory_space_constraint(x, pltpu.HBM) for x in operands]
    result = pl.pallas_call(
        functools.partial(kernel, devices),
        out_shape=pltpu.VMEM((count, half), bf16),
        in_specs=[hbm] * len(operands),
        out_specs=vmem,
        scratch_shapes=[
            pltpu.SMEM(slots, jnp.int32),
            pltpu.SMEM(slots, jnp.int32),
            pltpu.VMEM((1, half), f32),
            pltpu.VMEM(trig.shape, f32),
            pltpu.SemaphoreType.DMA((4,)),
            pltpu.VMEM((count, LANES), f32),
            pltpu.VMEM((count, LANES), f32),
            pltpu.VMEM((QUERY_BLOCK, QUERY_BLOCK), bf16),
            pltpu.VMEM((QUERY_BLOCK, QUERY_BLOCK), bf16),
            pltpu.VMEM(row_data.shape, bf16),
            pltpu.VMEM(query_weight.shape, bf16),
            pltpu.VMEM((key_weight.shape[0], 2 * key_weight.shape[1]), bf16),
            pltpu.VMEM(out_weight.shape, bf16),
            pltpu.SemaphoreType.DMA((count // ROWS,)),
            pltpu.SemaphoreType.DMA((3,)),
            pltpu.SemaphoreType.DMA((heads_width // HEAD_DIM,)),
            pltpu.VMEM((count // KEY_BLOCK, KEY_BLOCK, 2 * LANES), bf16),
            pltpu.VMEM((devices * qblocks, KEY_BLOCK, 2 * LANES), bf16),
            pltpu.VMEM((devices * qblocks, KEY_BLOCK, 2 * LANES), bf16),
            pltpu.VMEM((count, heads_width), bf16),
            pltpu.VMEM((count, heads_width), bf16),
            pltpu.VMEM((count, heads_width), bf16),
            pltpu.VMEM(out_weight.shape, bf16),
            pltpu.VMEM((QUERY_BLOCK, 2 * half), bf16),
            pltpu.VMEM((ROWS, half), f32),
            pltpu.SemaphoreType.DMA((qblocks, devices)),
            pltpu.SemaphoreType.DMA((qblocks, devices)),
            pltpu.SemaphoreType.DMA((2,)),
            pltpu.SemaphoreType.DMA((qblocks,)),
            pltpu.SemaphoreType.DMA((qblocks,)),
        ],
        compiler_params=pltpu.CompilerParams(
            collective_id=0, has_side_effects=True, vmem_limit_bytes=48 * 1024 * 1024
        ),
    )(*operands)
    return pl.pallas_call(
        store_kernel,
        out_shape=jax.ShapeDtypeStruct((count, half), bf16),
        in_specs=[vmem],
        out_specs=hbm,
        scratch_shapes=[pltpu.SemaphoreType.DMA((qblocks,))],
        compiler_params=pltpu.CompilerParams(vmem_limit_bytes=4 * 1024 * 1024),
    )(pltpu.with_memory_space_constraint(result, pltpu.VMEM))[None]


def solution(mesh):
    placed = (
        P("dp", "kv", None),
        P(None, "tp"),
        P(None, "tp"),
        P(None, "tp"),
        P("tp", None),
        P("tp"),
        P("dp", None, None),
        P("dp", None, None),
    )
    return jax.shard_map(
        body, mesh=mesh, in_specs=placed, out_specs=P("dp", "kv", "tp"), check_vma=False
    )
```

time: 29.7 us -> 28.9 us (0.973)
  the two profiles are of different devices: /device:TPU:29 before, /device:TPU:23 now
where the time goes in v2:
time: 28.9 us; the launch traced here: 28.8 us
  Pallas kernels  28.8 us (100%)
    pallas_call x1, Pallas kernels, body(): pl.pallas_call(functools.partial(kernel, devices), out_shape=pltpu.VMEM((...  27.6 us
    pallas_call x1, Pallas kernels, body(): pl.pallas_call(store_kernel, out_shape=jax.ShapeDtypeStruct((count, half)...  1.19 us

profile of v2, /device:TPU:23, one launch (start us, length us, event | category | flops | bytes accessed | tf_op | source)
XLA Modules:
  0.0 28.8 jit_solution(12167161266929457063)
XLA Ops:
  0.0 27.6 %shard_map.91.held = bf16[768,1024]{1,0:T(8,128)(2,1)S(1)} custom-call(s32[4,24]{1,0:T(4,128)} %bitcast.11, s32[4,24]{1,0:T(4,128)} %bitcast.12, bf16[768,2048]{1,0:T(8,128)(2,1)} %bitcast.9, bf16[2048,512]{1,0:T(8,128)(2,1)} %wq_hbm.1, bf16[2048,128]{1,0:T(8,128)(2,1)} %wk_hbm.1, bf16[2048,128]{1,0:T(8,128)(2,1)} %wv_hbm.1, bf16[512,2048]{1,0:T(8,128)(2,1)} %ow_hbm.1, ...), custom_call_target="tpu_custom_call" | custom-call | tf_op jit(solution)/shard_map/pallas_call | solution.py:408
  27.6 1.2 %shard_map.92 = bf16[768,1024]{1,0:T(8,128)(2,1)} custom-call(bf16[768,1024]{1,0:T(8,128)(2,1)S(1)} %shard_map.91.held), custom_call_target="tpu_custom_call" | custom-call | tf_op jit(solution)/shard_map/pallas_call | solution.py:449

commit v3 on v2

--- a/solution.py
+++ b/solution.py
@@ -37,9 +37,9 @@
 def kernel(
     devices, owner_hbm, part_hbm, tok_hbm, wq_hbm, wk_hbm, wv_hbm, ow_hbm, gain_hbm, trig_hbm, out,
     owner_ref, part_ref, gain, trig, small_sems, cosine, sine, eye, causal,
-    tok, wq, wkv, ow, tok_sems, weight_sems, ow_load_sems,
-    kv, send, pool, queries, mix, mix_other, ow_other, partial, proj,
-    kv_send, kv_recv, ow_sems, mix_send, mix_recv,
+    tok, wq, wkv, ow, tok_sems, weight_sems,
+    kv, send, pool, queries, keys_now, values_now, scores, weights, mix, mix_other, ow_other, partial, proj, ss, ss_other,
+    kv_send, kv_recv, ow_sems, mix_send, mix_recv, ss_send, ss_recv,
 ):
     me = lax.axis_index("kv")
     core = lax.axis_index("tp")
@@ -55,15 +55,17 @@
     heads = wq.shape[1] // HEAD_DIM
     bf16, f32 = jnp.bfloat16, jnp.float32
 
+    part_rows = tokens // 2
+
     def tok_copy(r):
-        rows = pl.ds(pl.multiple_of(r * ROWS, ROWS), ROWS)
+        rows = pl.ds(pl.multiple_of(r * part_rows, part_rows), part_rows)
         return pltpu.make_async_copy(tok_hbm.at[rows], tok.at[rows], tok_sems.at[r])
 
     wk_copy = pltpu.make_async_copy(wk_hbm, wkv.at[:, pl.ds(0, key_width)], weight_sems.at[0])
     wv_copy = pltpu.make_async_copy(
-        wv_hbm, wkv.at[:, pl.ds(key_width, key_width)], weight_sems.at[1]
+        wv_hbm, wkv.at[:, pl.ds(key_width, key_width)], weight_sems.at[0]
     )
-    wq_copy = pltpu.make_async_copy(wq_hbm, wq, weight_sems.at[2])
+    wq_copy = pltpu.make_async_copy(wq_hbm, wq, weight_sems.at[1])
     ow_loads = []
     for m in range(slices):
         for g in range(2):
@@ -71,7 +73,7 @@
                 pltpu.make_async_copy(
                     ow_hbm.at[pl.ds((g * slices + m) * HEAD_DIM, HEAD_DIM)],
                     ow.at[pl.ds((2 * m + g) * HEAD_DIM, HEAD_DIM)],
-                    ow_load_sems.at[2 * m + g],
+                    weight_sems.at[2],
                 )
             )
     small = [
@@ -83,10 +85,10 @@
     small[0].start()
     wk_copy.start()
     wv_copy.start()
-    for r in range(row_steps):
-        tok_copy(r).start()
+    tok_copy(0).start()
+    tok_copy(1).start(priority=1)
     for copy in small[1:]:
-        copy.start()
+        copy.start(priority=1)
 
     barrier = pltpu.get_barrier_semaphore()
 
@@ -102,7 +104,7 @@
     first = lax.broadcasted_iota(jnp.int32, square, 0)
     second = lax.broadcasted_iota(jnp.int32, square, 1)
     eye[...] = jnp.where(first == second, 1.0, 0.0).astype(bf16)
-    causal[...] = jnp.where(second >= first, 0.0, hidden).astype(bf16)
+    causal[...] = jnp.where(first >= second, 0.0, hidden).astype(bf16)
 
     small[0].wait()
     near_cos = trig[0:QUERY_BLOCK, :]
@@ -117,24 +119,23 @@
         cosine[rows, :] = far_cos * near_cos - far_sin * near_sin
         sine[rows, :] = far_sin * near_cos + far_cos * near_sin
 
-    wk_copy.wait()
-    wv_copy.wait()
-
-    @pl.loop(0, row_steps)
+    pltpu.make_async_copy(wkv, wkv, weight_sems.at[0]).wait()
+
+    @pl.loop(0, 2)
     def _(r):
         tok_copy(r).wait()
 
         @pl.when(r == 0)
         def _():
-            wq_copy.start()
+            wq_copy.start(priority=1)
             for copy in ow_loads:
-                copy.start()
-
-        rows = pl.ds(pl.multiple_of(r * ROWS, ROWS), ROWS)
+                copy.start(priority=1)
+
+        rows = pl.ds(pl.multiple_of(r * part_rows, part_rows), part_rows)
         both = jnp.dot(tok[rows, :], wkv[...], preferred_element_type=f32)
         keys = turn(both[:, :LANES], cosine[rows, :], sine[rows, :])
         joined = jnp.concatenate([keys, both[:, LANES:]], axis=1).astype(bf16)
-        blocks = ROWS // KEY_BLOCK
+        blocks = part_rows // KEY_BLOCK
         kv[pl.ds(r * blocks, blocks)] = joined.reshape(blocks, KEY_BLOCK, 2 * LANES)
 
     for copy in small[1:]:
@@ -150,10 +151,10 @@
 
     def kv_copy(src, dst, to, q):
         return pltpu.make_async_remote_copy(
-            src_ref=send.at[pl.ds(q * devices + dst, 1)],
+            src_ref=send.at[pl.ds(dst * qblocks + q, 1)],
             dst_ref=pool.at[pl.ds(q * devices + src, 1)],
-            send_sem=kv_send.at[q, dst],
-            recv_sem=kv_recv.at[q, src],
+            send_sem=kv_send.at[dst],
+            recv_sem=kv_recv.at[q],
             device_id={"kv": to},
             device_id_type=MESH,
         )
@@ -166,7 +167,7 @@
 
             @pl.when(dst > me)
             def _():
-                send[pl.ds(q * devices + dst, 1)] = kv[pl.ds(wanted(dst, q), 1)]
+                send[pl.ds(dst * qblocks + q, 1)] = kv[pl.ds(wanted(dst, q), 1)]
                 kv_copy(me, dst, dst, q).start()
 
     @pl.loop(0, qblocks)
@@ -193,8 +194,7 @@
     def _(r):
         @pl.when(r == 1)
         def _():
-            for copy in ow_loads:
-                copy.wait()
+            pltpu.make_async_copy(ow, ow, weight_sems.at[2]).wait()
             ow_copy.start()
 
         rows = pl.ds(pl.multiple_of(r * ROWS, ROWS), ROWS)
@@ -218,13 +218,24 @@
 
     key_count = devices * KEY_BLOCK + QUERY_BLOCK
 
+    blocks_in = ROWS // QUERY_BLOCK
+    last = qblocks - 1
+
+    def group_of(b):
+        return b // blocks_in + jnp.where(b == last, 1, 0)
+
+    def wait_mix(first, count):
+        rows = pl.ds(pl.multiple_of(first * QUERY_BLOCK, QUERY_BLOCK), count * QUERY_BLOCK)
+        landed = mix_other.at[rows]
+        pltpu.make_async_copy(landed, landed, mix_recv.at[group_of(first)]).wait()
+
     def mix_copy(b):
         rows = pl.ds(pl.multiple_of(b * QUERY_BLOCK, QUERY_BLOCK), QUERY_BLOCK)
         return pltpu.make_async_remote_copy(
             src_ref=mix.at[rows],
             dst_ref=mix_other.at[rows],
-            send_sem=mix_send.at[b],
-            recv_sem=mix_recv.at[b],
+            send_sem=mix_send.at[0],
+            recv_sem=mix_recv.at[group_of(b)],
             device_id={"tp": other},
             device_id_type=MESH,
         )
@@ -235,30 +246,32 @@
     def attend(b):
         row = me * qblocks + b
 
-        @pl.loop(0, devices)
-        def _(src):
-            @pl.when(src < me)
+        for n in range(1, devices):
+
+            @pl.when(me == n)
             def _():
-                kv_copy(src, src, src, b).wait_recv()
+                landed = pool.at[pl.ds(b * devices, n)]
+                pltpu.make_async_copy(landed, landed, kv_recv.at[b]).wait()
 
         rows = pl.ds(pl.multiple_of(b * QUERY_BLOCK, QUERY_BLOCK), QUERY_BLOCK)
         far = pool[pl.ds(b * devices, devices)].reshape(devices * KEY_BLOCK, 2 * LANES)
         near = kv[pl.ds(b * per_q, per_q)].reshape(QUERY_BLOCK, 2 * LANES)
         both = jnp.concatenate([far, near], axis=0)
         keys, values = both[:, :LANES], both[:, LANES:]
-        bias = []
-        for src in range(devices):
-            named = sum(jnp.where(place(src, row, s)[0], 1, 0) for s in range(chosen))
-            bias.append(
-                jnp.full((KEY_BLOCK, LANES), jnp.where(named > 0, 0.0, hidden), f32).astype(bf16)
-            )
-        bias = jnp.concatenate(bias + [causal[...]], axis=0)
+        owner = lax.broadcasted_iota(jnp.int32, (1, devices * KEY_BLOCK), 1) // KEY_BLOCK
+        bias = jnp.full((1, devices * KEY_BLOCK), hidden, f32)
+        for s in range(chosen):
+            bias = jnp.where(owner == owner_ref[s, row], 0.0, bias)
+        bias = jnp.broadcast_to(bias, (QUERY_BLOCK, devices * KEY_BLOCK)).astype(bf16)
+        bias = jnp.concatenate([bias, causal[...]], axis=1)
+        turned = keys.T
+        blank = jnp.zeros((HEAD_DIM, key_count), bf16)
         wide_keys = jnp.concatenate(
             [
-                jnp.concatenate([keys * low_mask, bias], axis=1),
-                jnp.concatenate([keys * high_mask, bias], axis=1),
+                jnp.concatenate([turned[:HEAD_DIM], blank, bias], axis=0),
+                jnp.concatenate([blank, turned[HEAD_DIM:], bias], axis=0),
             ],
-            axis=0,
+            axis=1,
         )
         wide_values = jnp.concatenate(
             [
@@ -267,101 +280,123 @@
             ],
             axis=0,
         )
-        for pair in range(0, slices, 2):
-            q = jnp.concatenate(
-                [
-                    jnp.concatenate([queries[rows, m * LANES : (m + 1) * LANES], eye[...]], axis=1)
-                    for m in (pair, pair + 1)
-                ],
-                axis=0,
+        keys_now[...] = wide_keys
+        values_now[...] = wide_values
+        sections = [slice(m * QUERY_BLOCK, (m + 1) * QUERY_BLOCK) for m in range(slices)]
+        for m, section in enumerate(sections):
+            q = jnp.concatenate([queries[rows, m * LANES : (m + 1) * LANES], eye[...]], axis=1)
+            scores[section, :] = jnp.dot(q, keys_now[...], preferred_element_type=f32)
+        for section in sections:
+            for side in range(2):
+                cols = slice(side * key_count, (side + 1) * key_count)
+                s = scores[section, cols]
+                weights[section, cols] = jnp.exp(s - jnp.max(s, axis=1, keepdims=True)).astype(bf16)
+        for m, section in enumerate(sections):
+            mixed = jnp.dot(weights[section, :], values_now[...], preferred_element_type=f32)
+            mix[rows, m * LANES : (m + 1) * LANES] = (mixed[:, :LANES] / mixed[:, LANES:]).astype(
+                bf16
             )
-            scores = lax.dot_general(
-                q, wide_keys, (((1,), (1,)), ((), ())), preferred_element_type=f32
-            )
-            weights = []
-            for side in range(2):
-                s = scores[:, side * key_count : (side + 1) * key_count]
-                weights.append(jnp.exp(s - jnp.max(s, axis=1, keepdims=True)).astype(bf16))
-            mixed = jnp.dot(
-                jnp.concatenate(weights, axis=1), wide_values, preferred_element_type=f32
-            )
-            mixed = (mixed[:, :LANES] / mixed[:, LANES:]).astype(bf16)
-            for k in range(2):
-                at = (pair + k) * LANES
-                mix[rows, at : at + LANES] = mixed[k * QUERY_BLOCK : (k + 1) * QUERY_BLOCK]
         mix_copy(b).start()
 
     def part_of(left, right, rows, side, c):
         cols = pl.ds(pl.multiple_of(side * half + c * COLS, COLS), COLS)
         return jnp.dot(left[rows, :], right[:, cols], preferred_element_type=f32).astype(bf16)
 
-    def project_mine(start, count):
-        rows = pl.ds(start, count)
-        for n, side in enumerate((other, core)):
-            for c in range(half // COLS):
-                at = n * half + c * COLS
-                partial[:count, at : at + COLS] = part_of(mix, ow, rows, side, c)
-
-    def project(start, count, ready=False):
-        rows = pl.ds(start, count)
-        total = jnp.zeros((count, LANES), f32)
-        for n, side in enumerate((other, core)):
-            for c in range(half // COLS):
-                at = n * half + c * COLS
-                mine = partial[:count, at : at + COLS] if ready else part_of(mix, ow, rows, side, c)
-                theirs = part_of(mix_other, ow_other, rows, side, c)
-                added = mine.astype(f32) + theirs.astype(f32)
-                if side is core:
-                    proj[:count, c * COLS : (c + 1) * COLS] = added
-                for k in range(COLS // LANES):
-                    piece = added[:, k * LANES : (k + 1) * LANES]
-                    total = total + piece * piece
+    def ss_copy(b):
+        return pltpu.make_async_remote_copy(
+            src_ref=ss.at[b],
+            dst_ref=ss_other.at[b],
+            send_sem=ss_send.at[0],
+            recv_sem=ss_recv.at[group_of(b)],
+            device_id={"tp": other},
+            device_id_type=MESH,
+        )
+
+    def squares(total, added):
+        for k in range(COLS // LANES):
+            piece = added[:, k * LANES : (k + 1) * LANES]
+            total = total + piece * piece
+        return total
+
+    def project(first, count):
+        wait_mix(first, count)
+        size = count * QUERY_BLOCK
+        rows = pl.ds(pl.multiple_of(first * QUERY_BLOCK, QUERY_BLOCK), size)
+        total = jnp.zeros((size, LANES), f32)
+        for c in range(half // COLS):
+            mine = part_of(mix, ow, rows, core, c)
+            theirs = part_of(mix_other, ow_other, rows, core, c)
+            added = mine.astype(f32) + theirs.astype(f32)
+            proj[rows, c * COLS : (c + 1) * COLS] = added
+            total = squares(total, added)
+        for j in range(count):
+            ss[first + j] = total[j * QUERY_BLOCK : (j + 1) * QUERY_BLOCK]
+            ss_copy(first + j).start()
+
+    def normed(rows, total):
         scale = lax.rsqrt(jnp.sum(total, axis=1, keepdims=True) / (2 * half) + norm_eps)
         for c in range(half // LANES):
             at = slice(c * LANES, (c + 1) * LANES)
-            out[rows, at] = (proj[:count, at] * scale * gain[:, at]).astype(bf16)
-
-    blocks_in = ROWS // QUERY_BLOCK
-
-    @pl.loop(0, row_steps)
-    def _(r):
-        @pl.loop(0, blocks_in)
-        def _(k):
-            attend(r * blocks_in + k)
-
-            @pl.when(jnp.logical_and(r == 1, k == 0))
-            def _():
-                ow_copy.wait_recv()
-
-            @pl.when(jnp.logical_and(r > 0, k == 0))
-            def _():
-                for j in range(blocks_in):
-                    mix_copy((r - 1) * blocks_in + j).wait_recv()
-                project(pl.multiple_of((r - 1) * ROWS, ROWS), ROWS)
-
-    for b in range(qblocks - blocks_in, qblocks - 1):
-        mix_copy(b).wait_recv()
-        project(b * QUERY_BLOCK, QUERY_BLOCK)
-    last = qblocks - 1
-    project_mine(last * QUERY_BLOCK, QUERY_BLOCK)
+            out[rows, at] = (proj[rows, at] * scale * gain[:, at]).astype(bf16)
+
+    def norm(first, count):
+        landed = ss_other.at[pl.ds(first, count)]
+        pltpu.make_async_copy(landed, landed, ss_recv.at[group_of(first)]).wait()
+
+        @pl.loop(0, count)
+        def _(j):
+            b = first + j
+            rows = pl.ds(pl.multiple_of(b * QUERY_BLOCK, QUERY_BLOCK), QUERY_BLOCK)
+            normed(rows, ss[b] + ss_other[b])
 
     @pl.loop(0, qblocks)
-    def _(q):
-        @pl.loop(0, devices)
-        def _(dst):
-            @pl.when(dst > me)
-            def _():
-                kv_copy(me, dst, dst, q).wait_send()
+    def _(b):
+        attend(b)
+
+        @pl.when(b == 1)
+        def _():
+            ow_copy.wait_recv()
+
+        late = jnp.logical_and(b >= 2 * blocks_in, b % blocks_in == 0)
+
+        @pl.when(jnp.logical_or(b == blocks_in - 1, late))
+        def _():
+            project(jnp.where(late, b - blocks_in, 0), blocks_in)
+
+        @pl.when(late)
+        def _():
+            norm(b - 2 * blocks_in, blocks_in)
+
+    project(last - 1, 1)
+    norm(last - 1 - blocks_in, blocks_in)
+    final = slice(last * QUERY_BLOCK, qblocks * QUERY_BLOCK)
+    for n, side in enumerate((other, core)):
+        for c in range(half // COLS):
+            at = n * half + c * COLS
+            partial[:, at : at + COLS] = part_of(mix, ow, final, side, c)
+
+    @pl.loop(0, devices)
+    def _(dst):
+        @pl.when(dst > me)
+        def _():
+            sent = send.at[pl.ds(dst * qblocks, qblocks)]
+            pltpu.make_async_copy(sent, sent, kv_send.at[dst]).wait()
 
     ow_copy.wait_send()
-
-    @pl.loop(0, last)
-    def _(b):
-        mix_copy(b).wait_send()
-
-    mix_copy(last).wait_recv()
-    project(last * QUERY_BLOCK, QUERY_BLOCK, ready=True)
-    mix_copy(last).wait_send()
+    pltpu.make_async_copy(ss.at[pl.ds(0, last)], ss.at[pl.ds(0, last)], ss_send.at[0]).wait()
+    norm(last - 1, 1)
+    wait_mix(last, 1)
+    total = jnp.zeros((QUERY_BLOCK, LANES), f32)
+    for n, side in enumerate((other, core)):
+        for c in range(half // COLS):
+            at = n * half + c * COLS
+            theirs = part_of(mix_other, ow_other, final, side, c)
+            added = partial[:, at : at + COLS].astype(f32) + theirs.astype(f32)
+            if side is core:
+                proj[final, c * COLS : (c + 1) * COLS] = added
+            total = squares(total, added)
+    normed(final, total)
+    pltpu.make_async_copy(mix, mix, mix_send.at[0]).wait()
 
 
 def store_kernel(held, out, sems):
@@ -399,6 +434,7 @@
     vmem = pl.BlockSpec(memory_space=pltpu.VMEM)
     bf16, f32 = jnp.bfloat16, jnp.float32
     slots = chosen_owner.shape[1:][::-1]
+    key_count = devices * KEY_BLOCK + QUERY_BLOCK
     trig = trig_table(devices * qblocks)
     operands = [
         chosen_owner[0].T, chosen_part[0].T, row_data, query_weight, key_weight, value_weight,
@@ -424,23 +460,30 @@
             pltpu.VMEM(query_weight.shape, bf16),
             pltpu.VMEM((key_weight.shape[0], 2 * key_weight.shape[1]), bf16),
             pltpu.VMEM(out_weight.shape, bf16),
-            pltpu.SemaphoreType.DMA((count // ROWS,)),
+            pltpu.SemaphoreType.DMA((2,)),
             pltpu.SemaphoreType.DMA((3,)),
-            pltpu.SemaphoreType.DMA((heads_width // HEAD_DIM,)),
             pltpu.VMEM((count // KEY_BLOCK, KEY_BLOCK, 2 * LANES), bf16),
             pltpu.VMEM((devices * qblocks, KEY_BLOCK, 2 * LANES), bf16),
             pltpu.VMEM((devices * qblocks, KEY_BLOCK, 2 * LANES), bf16),
             pltpu.VMEM((count, heads_width), bf16),
+            pltpu.VMEM((LANES + QUERY_BLOCK, 2 * key_count), bf16),
+            pltpu.VMEM((2 * key_count, 2 * LANES), bf16),
+            pltpu.VMEM((heads_width // LANES * QUERY_BLOCK, 2 * key_count), f32),
+            pltpu.VMEM((heads_width // LANES * QUERY_BLOCK, 2 * key_count), bf16),
             pltpu.VMEM((count, heads_width), bf16),
             pltpu.VMEM((count, heads_width), bf16),
             pltpu.VMEM(out_weight.shape, bf16),
             pltpu.VMEM((QUERY_BLOCK, 2 * half), bf16),
-            pltpu.VMEM((ROWS, half), f32),
-            pltpu.SemaphoreType.DMA((qblocks, devices)),
-            pltpu.SemaphoreType.DMA((qblocks, devices)),
+            pltpu.VMEM((count, half), f32),
+            pltpu.VMEM((qblocks, QUERY_BLOCK, LANES), f32),
+            pltpu.VMEM((qblocks, QUERY_BLOCK, LANES), f32),
+            pltpu.SemaphoreType.DMA((devices,)),
+            pltpu.SemaphoreType.DMA((qblocks,)),
             pltpu.SemaphoreType.DMA((2,)),
-            pltpu.SemaphoreType.DMA((qblocks,)),
-            pltpu.SemaphoreType.DMA((qblocks,)),
+            pltpu.SemaphoreType.DMA((1,)),
+            pltpu.SemaphoreType.DMA((count // ROWS + 1,)),
+            pltpu.SemaphoreType.DMA((1,)),
+            pltpu.SemaphoreType.DMA((count // ROWS,)),
         ],
         compiler_params=pltpu.CompilerParams(
             collective_id=0, has_side_effects=True, vmem_limit_bytes=48 * 1024 * 1024

time: 28.9 us -> 26.9 us (0.931)
  Pallas kernels: 28.8 us -> 26.8 us
    pallas_call x1, Pallas kernels: 27.6 us -> 25.6 us  [body(): pl.pallas_call(functools.partial(kernel, devices), out_shape=pltpu.VMEM((...]
where the time goes in v3:
time: 26.9 us; the launch traced here: 26.8 us
  Pallas kernels  26.8 us (100%)
    pallas_call x1, Pallas kernels, body(): pl.pallas_call(functools.partial(kernel, devices), out_shape=pltpu.VMEM((...  25.6 us
    pallas_call x1, Pallas kernels, body(): pl.pallas_call(store_kernel, out_shape=jax.ShapeDtypeStruct((count, half)...  1.19 us

profile of v3, /device:TPU:23, one launch (start us, length us, event | category | flops | bytes accessed | tf_op | source)
XLA Modules:
  0.0 26.8 jit_solution(12978703357951296820)
XLA Ops:
  0.0 25.6 %shard_map.91.held = bf16[768,1024]{1,0:T(8,128)(2,1)S(1)} custom-call(s32[4,24]{1,0:T(4,128)} %bitcast.11, s32[4,24]{1,0:T(4,128)} %bitcast.12, bf16[768,2048]{1,0:T(8,128)(2,1)} %bitcast.9, bf16[2048,512]{1,0:T(8,128)(2,1)} %wq_hbm.1, bf16[2048,128]{1,0:T(8,128)(2,1)} %wk_hbm.1, bf16[2048,128]{1,0:T(8,128)(2,1)} %wv_hbm.1, bf16[512,2048]{1,0:T(8,128)(2,1)} %ow_hbm.1, ...), custom_call_target="tpu_custom_call" | custom-call | tf_op jit(solution)/shard_map/pallas_call | solution.py:444
  25.6 1.2 %shard_map.92 = bf16[768,1024]{1,0:T(8,128)(2,1)} custom-call(bf16[768,1024]{1,0:T(8,128)(2,1)S(1)} %shard_map.91.held), custom_call_target="tpu_custom_call" | custom-call | tf_op jit(solution)/shard_map/pallas_call | solution.py:492

commit v4 on v3

--- a/solution.py
+++ b/solution.py
@@ -149,18 +149,22 @@
         found = [place(me, dst * qblocks + q, s) for s in range(chosen)]
         return sum(jnp.where(here, at, 0) for here, at in found)
 
-    def kv_copy(src, dst, to, q):
+    def kv_copy(dst, q, lanes, sem):
         return pltpu.make_async_remote_copy(
-            src_ref=send.at[pl.ds(dst * qblocks + q, 1)],
-            dst_ref=pool.at[pl.ds(q * devices + src, 1)],
+            src_ref=send.at[pl.ds(dst * qblocks + q, 1), :, lanes],
+            dst_ref=pool.at[pl.ds(q * devices + me, 1), :, lanes],
             send_sem=kv_send.at[dst],
-            recv_sem=kv_recv.at[q],
-            device_id={"kv": to},
+            recv_sem=kv_recv.at[sem],
+            device_id={"kv": dst},
             device_id_type=MESH,
         )
 
-    @pl.loop(0, qblocks)
-    def _(q):
+    last = qblocks - 1
+    all_lanes, key_lanes, value_lanes = (
+        pl.ds(0, 2 * LANES), pl.ds(0, LANES), pl.ds(LANES, LANES)
+    )
+
+    def send_block(q, split):
         @pl.loop(0, devices - 1)
         def _(step):
             dst = devices - 1 - step
@@ -168,7 +172,27 @@
             @pl.when(dst > me)
             def _():
                 send[pl.ds(dst * qblocks + q, 1)] = kv[pl.ds(wanted(dst, q), 1)]
-                kv_copy(me, dst, dst, q).start()
+                kv_copy(dst, q, key_lanes if split else all_lanes, q).start()
+
+        if split:
+
+            @pl.loop(0, devices - 1)
+            def _(step):
+                dst = devices - 1 - step
+
+                @pl.when(dst > me)
+                def _():
+                    kv_copy(dst, q, value_lanes, qblocks).start()
+
+    paced = me + 3 < devices
+
+    @pl.loop(0, jnp.where(paced, 1, last))
+    def _(q):
+        send_block(q, False)
+
+    @pl.when(jnp.logical_not(paced))
+    def _():
+        send_block(last, True)
 
     @pl.loop(0, qblocks)
     def _(q):
@@ -192,6 +216,10 @@
 
     @pl.loop(0, row_steps)
     def _(r):
+        @pl.when(jnp.logical_and(paced, r == row_steps - 1))
+        def _():
+            send_block(1, False)
+
         @pl.when(r == 1)
         def _():
             pltpu.make_async_copy(ow, ow, weight_sems.at[2]).wait()
@@ -219,7 +247,6 @@
     key_count = devices * KEY_BLOCK + QUERY_BLOCK
 
     blocks_in = ROWS // QUERY_BLOCK
-    last = qblocks - 1
 
     def group_of(b):
         return b // blocks_in + jnp.where(b == last, 1, 0)
@@ -243,21 +270,25 @@
     low_mask = jnp.where(low_lanes((key_count, LANES)), 1.0, 0.0).astype(bf16)
     high_mask = jnp.where(low_lanes((key_count, LANES)), 0.0, 1.0).astype(bf16)
 
-    def attend(b):
-        row = me * qblocks + b
-
+    def wait_kv(b, lanes, sem):
         for n in range(1, devices):
 
             @pl.when(me == n)
             def _():
-                landed = pool.at[pl.ds(b * devices, n)]
-                pltpu.make_async_copy(landed, landed, kv_recv.at[b]).wait()
-
+                landed = pool.at[pl.ds(b * devices, n), :, lanes]
+                pltpu.make_async_copy(landed, landed, kv_recv.at[sem]).wait()
+
+    def block_of(b, lanes):
+        far = pool[pl.ds(b * devices, devices), :, lanes].reshape(devices * KEY_BLOCK, LANES)
+        near = kv[pl.ds(b * per_q, per_q), :, lanes].reshape(QUERY_BLOCK, LANES)
+        return jnp.concatenate([far, near], axis=0)
+
+    sections = [slice(m * QUERY_BLOCK, (m + 1) * QUERY_BLOCK) for m in range(slices)]
+
+    def attend_keys(b):
+        row = me * qblocks + b
         rows = pl.ds(pl.multiple_of(b * QUERY_BLOCK, QUERY_BLOCK), QUERY_BLOCK)
-        far = pool[pl.ds(b * devices, devices)].reshape(devices * KEY_BLOCK, 2 * LANES)
-        near = kv[pl.ds(b * per_q, per_q)].reshape(QUERY_BLOCK, 2 * LANES)
-        both = jnp.concatenate([far, near], axis=0)
-        keys, values = both[:, :LANES], both[:, LANES:]
+        keys = block_of(b, slice(0, LANES))
         owner = lax.broadcasted_iota(jnp.int32, (1, devices * KEY_BLOCK), 1) // KEY_BLOCK
         bias = jnp.full((1, devices * KEY_BLOCK), hidden, f32)
         for s in range(chosen):
@@ -273,16 +304,7 @@
             ],
             axis=1,
         )
-        wide_values = jnp.concatenate(
-            [
-                jnp.concatenate([values * low_mask, low_mask], axis=1),
-                jnp.concatenate([values * high_mask, high_mask], axis=1),
-            ],
-            axis=0,
-        )
         keys_now[...] = wide_keys
-        values_now[...] = wide_values
-        sections = [slice(m * QUERY_BLOCK, (m + 1) * QUERY_BLOCK) for m in range(slices)]
         for m, section in enumerate(sections):
             q = jnp.concatenate([queries[rows, m * LANES : (m + 1) * LANES], eye[...]], axis=1)
             scores[section, :] = jnp.dot(q, keys_now[...], preferred_element_type=f32)
@@ -291,6 +313,17 @@
                 cols = slice(side * key_count, (side + 1) * key_count)
                 s = scores[section, cols]
                 weights[section, cols] = jnp.exp(s - jnp.max(s, axis=1, keepdims=True)).astype(bf16)
+
+    def attend_values(b):
+        rows = pl.ds(pl.multiple_of(b * QUERY_BLOCK, QUERY_BLOCK), QUERY_BLOCK)
+        values = block_of(b, slice(LANES, 2 * LANES))
+        values_now[...] = jnp.concatenate(
+            [
+                jnp.concatenate([values * low_mask, low_mask], axis=1),
+                jnp.concatenate([values * high_mask, high_mask], axis=1),
+            ],
+            axis=0,
+        )
         for m, section in enumerate(sections):
             mixed = jnp.dot(weights[section, :], values_now[...], preferred_element_type=f32)
             mix[rows, m * LANES : (m + 1) * LANES] = (mixed[:, :LANES] / mixed[:, LANES:]).astype(
@@ -349,26 +382,41 @@
             rows = pl.ds(pl.multiple_of(b * QUERY_BLOCK, QUERY_BLOCK), QUERY_BLOCK)
             normed(rows, ss[b] + ss_other[b])
 
-    @pl.loop(0, qblocks)
+    @pl.loop(0, last)
     def _(b):
-        attend(b)
+        wait_kv(b, all_lanes, b)
+        attend_keys(b)
+        attend_values(b)
 
         @pl.when(b == 1)
         def _():
             ow_copy.wait_recv()
 
-        late = jnp.logical_and(b >= 2 * blocks_in, b % blocks_in == 0)
-
-        @pl.when(jnp.logical_or(b == blocks_in - 1, late))
-        def _():
-            project(jnp.where(late, b - blocks_in, 0), blocks_in)
-
-        @pl.when(late)
-        def _():
-            norm(b - 2 * blocks_in, blocks_in)
+        @pl.when(jnp.logical_and(paced, jnp.logical_and(b > 0, b < last - 2)))
+        def _():
+            send_block(b + 1, False)
+
+        @pl.when(b % blocks_in == blocks_in - 1)
+        def _():
+            project(b + 1 - blocks_in, blocks_in)
+
+        @pl.when(jnp.logical_and(paced, b == last - 2))
+        def _():
+            send_block(last - 1, False)
+
+        @pl.when(jnp.logical_and(b > 0, b % blocks_in == 0))
+        def _():
+            norm(b - blocks_in, blocks_in)
+
+    @pl.when(paced)
+    def _():
+        send_block(last, True)
 
     project(last - 1, 1)
-    norm(last - 1 - blocks_in, blocks_in)
+    wait_kv(last, key_lanes, last)
+    attend_keys(last)
+    wait_kv(last, value_lanes, qblocks)
+    attend_values(last)
     final = slice(last * QUERY_BLOCK, qblocks * QUERY_BLOCK)
     for n, side in enumerate((other, core)):
         for c in range(half // COLS):
@@ -478,7 +526,7 @@
             pltpu.VMEM((qblocks, QUERY_BLOCK, LANES), f32),
             pltpu.VMEM((qblocks, QUERY_BLOCK, LANES), f32),
             pltpu.SemaphoreType.DMA((devices,)),
-            pltpu.SemaphoreType.DMA((qblocks,)),
+            pltpu.SemaphoreType.DMA((qblocks + 1,)),
             pltpu.SemaphoreType.DMA((2,)),
             pltpu.SemaphoreType.DMA((1,)),
             pltpu.SemaphoreType.DMA((count // ROWS + 1,)),

time: 26.9 us -> 25.7 us (0.955)
  Pallas kernels: 26.8 us -> 25.5 us
    pallas_call x1, Pallas kernels: 25.6 us -> 24.3 us  [body(): pl.pallas_call(functools.partial(kernel, devices), out_shape=pltpu.VMEM((...]
where the time goes in v4:
time: 25.7 us; the launch traced here: 25.5 us
  Pallas kernels  25.5 us (99%)
    pallas_call x1, Pallas kernels, body(): pl.pallas_call(functools.partial(kernel, devices), out_shape=pltpu.VMEM((...  24.3 us
    pallas_call x1, Pallas kernels, body(): pl.pallas_call(store_kernel, out_shape=jax.ShapeDtypeStruct((count, half)...  1.19 us

profile of v4, /device:TPU:23, one launch (start us, length us, event | category | flops | bytes accessed | tf_op | source)
XLA Modules:
  0.0 25.5 jit_solution(4176864989968638483)
XLA Ops:
  0.0 24.3 %shard_map.91.held = bf16[768,1024]{1,0:T(8,128)(2,1)S(1)} custom-call(s32[4,24]{1,0:T(4,128)} %bitcast.11, s32[4,24]{1,0:T(4,128)} %bitcast.12, bf16[768,2048]{1,0:T(8,128)(2,1)} %bitcast.9, bf16[2048,512]{1,0:T(8,128)(2,1)} %wq_hbm.1, bf16[2048,128]{1,0:T(8,128)(2,1)} %wk_hbm.1, bf16[2048,128]{1,0:T(8,128)(2,1)} %wv_hbm.1, bf16[512,2048]{1,0:T(8,128)(2,1)} %ow_hbm.1, ...), custom_call_target="tpu_custom_call" | custom-call | tf_op jit(solution)/shard_map/pallas_call | solution.py:492
  24.4 1.2 %shard_map.92 = bf16[768,1024]{1,0:T(8,128)(2,1)} custom-call(bf16[768,1024]{1,0:T(8,128)(2,1)S(1)} %shard_map.91.held), custom_call_target="tpu_custom_call" | custom-call | tf_op jit(solution)/shard_map/pallas_call | solution.py:540

commit v5 on v4

--- a/solution.py
+++ b/solution.py
@@ -34,11 +34,29 @@
     return u * cosine + swapped * sine
 
 
+def part_of(left, right, rows, half, side, c):
+    cols = pl.ds(pl.multiple_of(side * half + c * COLS, COLS), COLS)
+    return jnp.dot(
+        left[rows, :], right[:, cols], preferred_element_type=jnp.float32
+    ).astype(jnp.bfloat16)
+
+
+def squares(total, added):
+    for k in range(COLS // LANES):
+        piece = added[:, k * LANES : (k + 1) * LANES]
+        total = total + piece * piece
+    return total
+
+
+def row_scale(total, half):
+    return lax.rsqrt(jnp.sum(total, axis=1, keepdims=True) / (2 * half) + norm_eps)
+
+
 def kernel(
-    devices, owner_hbm, part_hbm, tok_hbm, wq_hbm, wk_hbm, wv_hbm, ow_hbm, gain_hbm, trig_hbm, out,
-    owner_ref, part_ref, gain, trig, small_sems, cosine, sine, eye, causal,
+    devices, owner_hbm, part_hbm, tok_hbm, wq_hbm, wk_hbm, wv_hbm, ow_hbm, gain_hbm, near_hbm, far_hbm, out, mix_end, ow_other, partial, gain_end,
+    owner_ref, part_ref, gain, near_trig, far_trig, small_sems, cosine, sine, eye, causal,
     tok, wq, wkv, ow, tok_sems, weight_sems,
-    kv, send, pool, queries, keys_now, values_now, scores, weights, mix, mix_other, ow_other, partial, proj, ss, ss_other,
+    kv, send, pool, queries, keys_now, values_now, scores, weights, mix, mix_other, early, proj, ss, ss_other,
     kv_send, kv_recv, ow_sems, mix_send, mix_recv, ss_send, ss_recv,
 ):
     me = lax.axis_index("kv")
@@ -55,10 +73,10 @@
     heads = wq.shape[1] // HEAD_DIM
     bf16, f32 = jnp.bfloat16, jnp.float32
 
-    part_rows = tokens // 2
+    pieces = ((0, ROWS), (ROWS, tokens - ROWS))
 
     def tok_copy(r):
-        rows = pl.ds(pl.multiple_of(r * part_rows, part_rows), part_rows)
+        rows = pl.ds(*pieces[r])
         return pltpu.make_async_copy(tok_hbm.at[rows], tok.at[rows], tok_sems.at[r])
 
     wk_copy = pltpu.make_async_copy(wk_hbm, wkv.at[:, pl.ds(0, key_width)], weight_sems.at[0])
@@ -77,17 +95,19 @@
                 )
             )
     small = [
-        pltpu.make_async_copy(trig_hbm, trig, small_sems.at[0]),
+        pltpu.make_async_copy(near_hbm, near_trig, small_sems.at[0]),
+        pltpu.make_async_copy(far_hbm.at[me], far_trig, small_sems.at[4]),
         pltpu.make_async_copy(owner_hbm, owner_ref, small_sems.at[1]),
         pltpu.make_async_copy(part_hbm, part_ref, small_sems.at[2]),
         pltpu.make_async_copy(gain_hbm, gain, small_sems.at[3]),
     ]
     small[0].start()
+    small[1].start()
     wk_copy.start()
     wv_copy.start()
     tok_copy(0).start()
     tok_copy(1).start(priority=1)
-    for copy in small[1:]:
+    for copy in small[2:]:
         copy.start(priority=1)
 
     barrier = pltpu.get_barrier_semaphore()
@@ -107,38 +127,38 @@
     causal[...] = jnp.where(first >= second, 0.0, hidden).astype(bf16)
 
     small[0].wait()
-    near_cos = trig[0:QUERY_BLOCK, :]
-    near_sin = trig[QUERY_BLOCK : 2 * QUERY_BLOCK, :]
+    small[1].wait()
+    near_cos = near_trig[0:QUERY_BLOCK, :]
+    near_sin = near_trig[QUERY_BLOCK : 2 * QUERY_BLOCK, :]
 
     @pl.loop(0, qblocks)
     def _(b):
         rows = pl.ds(pl.multiple_of(b * QUERY_BLOCK, QUERY_BLOCK), QUERY_BLOCK)
-        at = 2 * QUERY_BLOCK + me * qblocks + b
-        far_cos = trig[pl.ds(at, 1), :]
-        far_sin = trig[pl.ds(at + devices * qblocks, 1), :]
+        far_cos = far_trig[pl.ds(b, 1), :]
+        far_sin = far_trig[pl.ds(b + qblocks, 1), :]
         cosine[rows, :] = far_cos * near_cos - far_sin * near_sin
         sine[rows, :] = far_sin * near_cos + far_cos * near_sin
 
     pltpu.make_async_copy(wkv, wkv, weight_sems.at[0]).wait()
 
-    @pl.loop(0, 2)
-    def _(r):
-        tok_copy(r).wait()
-
-        @pl.when(r == 0)
-        def _():
-            wq_copy.start(priority=1)
-            for copy in ow_loads:
-                copy.start(priority=1)
-
-        rows = pl.ds(pl.multiple_of(r * part_rows, part_rows), part_rows)
-        both = jnp.dot(tok[rows, :], wkv[...], preferred_element_type=f32)
-        keys = turn(both[:, :LANES], cosine[rows, :], sine[rows, :])
-        joined = jnp.concatenate([keys, both[:, LANES:]], axis=1).astype(bf16)
-        blocks = part_rows // KEY_BLOCK
-        kv[pl.ds(r * blocks, blocks)] = joined.reshape(blocks, KEY_BLOCK, 2 * LANES)
-
-    for copy in small[1:]:
+    once = jnp.where(core >= 0, 1, 0)
+    for r, (start, size) in enumerate(pieces):
+
+        @pl.loop(0, once)
+        def _(_):
+            tok_copy(r).wait()
+            if r == 0:
+                wq_copy.start(priority=1)
+                for copy in ow_loads:
+                    copy.start(priority=1)
+            rows = pl.ds(start, size)
+            both = jnp.dot(tok[rows, :], wkv[...], preferred_element_type=f32)
+            keys = turn(both[:, :LANES], cosine[rows, :], sine[rows, :])
+            joined = jnp.concatenate([keys, both[:, LANES:]], axis=1).astype(bf16)
+            blocks = size // KEY_BLOCK
+            kv[pl.ds(start // KEY_BLOCK, blocks)] = joined.reshape(blocks, KEY_BLOCK, 2 * LANES)
+
+    for copy in small[2:]:
         copy.wait()
     pl.semaphore_wait(barrier, devices)
 
@@ -260,7 +280,7 @@
         rows = pl.ds(pl.multiple_of(b * QUERY_BLOCK, QUERY_BLOCK), QUERY_BLOCK)
         return pltpu.make_async_remote_copy(
             src_ref=mix.at[rows],
-            dst_ref=mix_other.at[rows],
+            dst_ref=mix_other.at[rows] if b is not last else mix_end,
             send_sem=mix_send.at[0],
             recv_sem=mix_recv.at[group_of(b)],
             device_id={"tp": other},
@@ -331,10 +351,6 @@
             )
         mix_copy(b).start()
 
-    def part_of(left, right, rows, side, c):
-        cols = pl.ds(pl.multiple_of(side * half + c * COLS, COLS), COLS)
-        return jnp.dot(left[rows, :], right[:, cols], preferred_element_type=f32).astype(bf16)
-
     def ss_copy(b):
         return pltpu.make_async_remote_copy(
             src_ref=ss.at[b],
@@ -345,29 +361,29 @@
             device_id_type=MESH,
         )
 
-    def squares(total, added):
-        for k in range(COLS // LANES):
-            piece = added[:, k * LANES : (k + 1) * LANES]
-            total = total + piece * piece
-        return total
-
-    def project(first, count):
+    def project_mine(first):
+        rows = pl.ds(pl.multiple_of(first * QUERY_BLOCK, QUERY_BLOCK), QUERY_BLOCK)
+        for c in range(half // COLS):
+            early[:, c * COLS : (c + 1) * COLS] = part_of(mix, ow, rows, half, core, c)
+
+    def project(first, count, ready=False):
         wait_mix(first, count)
         size = count * QUERY_BLOCK
         rows = pl.ds(pl.multiple_of(first * QUERY_BLOCK, QUERY_BLOCK), size)
         total = jnp.zeros((size, LANES), f32)
         for c in range(half // COLS):
-            mine = part_of(mix, ow, rows, core, c)
-            theirs = part_of(mix_other, ow_other, rows, core, c)
+            at = slice(c * COLS, (c + 1) * COLS)
+            mine = early[:, at] if ready else part_of(mix, ow, rows, half, core, c)
+            theirs = part_of(mix_other, ow_other, rows, half, core, c)
             added = mine.astype(f32) + theirs.astype(f32)
-            proj[rows, c * COLS : (c + 1) * COLS] = added
+            proj[rows, at] = added
             total = squares(total, added)
         for j in range(count):
             ss[first + j] = total[j * QUERY_BLOCK : (j + 1) * QUERY_BLOCK]
             ss_copy(first + j).start()
 
     def normed(rows, total):
-        scale = lax.rsqrt(jnp.sum(total, axis=1, keepdims=True) / (2 * half) + norm_eps)
+        scale = row_scale(total, half)
         for c in range(half // LANES):
             at = slice(c * LANES, (c + 1) * LANES)
             out[rows, at] = (proj[rows, at] * scale * gain[:, at]).astype(bf16)
@@ -412,16 +428,18 @@
     def _():
         send_block(last, True)
 
-    project(last - 1, 1)
+    project_mine(last - 1)
+    gain_end[...] = gain[...]
     wait_kv(last, key_lanes, last)
     attend_keys(last)
     wait_kv(last, value_lanes, qblocks)
     attend_values(last)
+    project(last - 1, 1, ready=True)
     final = slice(last * QUERY_BLOCK, qblocks * QUERY_BLOCK)
     for n, side in enumerate((other, core)):
         for c in range(half // COLS):
             at = n * half + c * COLS
-            partial[:, at : at + COLS] = part_of(mix, ow, final, side, c)
+            partial[:, at : at + COLS] = part_of(mix, ow, final, half, side, c)
 
     @pl.loop(0, devices)
     def _(dst):
@@ -432,41 +450,50 @@
 
     ow_copy.wait_send()
     pltpu.make_async_copy(ss.at[pl.ds(0, last)], ss.at[pl.ds(0, last)], ss_send.at[0]).wait()
+    pltpu.make_async_copy(mix_end, mix_end, mix_recv.at[group_of(last)]).wait()
+    pltpu.make_async_copy(mix, mix, mix_send.at[0]).wait()
     norm(last - 1, 1)
-    wait_mix(last, 1)
-    total = jnp.zeros((QUERY_BLOCK, LANES), f32)
-    for n, side in enumerate((other, core)):
+
+
+def finish_kernel(held, mix_end, ow_other, partial, gain, out, proj, end, sems):
+    core = lax.axis_index("tp")
+    half = gain.shape[1]
+    early = held.shape[0] - QUERY_BLOCK
+    rows = pl.ds(0, early)
+    first = pltpu.make_async_copy(held.at[rows], out.at[rows], sems.at[0])
+    first.start()
+    every = slice(0, QUERY_BLOCK)
+    total = jnp.zeros((QUERY_BLOCK, LANES), jnp.float32)
+    for n, side in enumerate((1 - core, core)):
         for c in range(half // COLS):
             at = n * half + c * COLS
-            theirs = part_of(mix_other, ow_other, final, side, c)
-            added = partial[:, at : at + COLS].astype(f32) + theirs.astype(f32)
+            theirs = part_of(mix_end, ow_other, every, half, side, c)
+            mine = partial[:, at : at + COLS]
+            added = mine.astype(jnp.float32) + theirs.astype(jnp.float32)
             if side is core:
-                proj[final, c * COLS : (c + 1) * COLS] = added
+                proj[:, c * COLS : (c + 1) * COLS] = added
             total = squares(total, added)
-    normed(final, total)
-    pltpu.make_async_copy(mix, mix, mix_send.at[0]).wait()
-
-
-def store_kernel(held, out, sems):
-    def copy(b):
-        rows = pl.ds(b * QUERY_BLOCK, QUERY_BLOCK)
-        return pltpu.make_async_copy(held.at[rows], out.at[rows], sems.at[b])
-
-    for b in range(sems.shape[0]):
-        copy(b).start()
-    for b in range(sems.shape[0]):
-        copy(b).wait()
-
-
-def trig_table(blocks):
+    scale = row_scale(total, half)
+    for c in range(half // LANES):
+        at = slice(c * LANES, (c + 1) * LANES)
+        end[:, at] = (proj[:, at] * scale * gain[:, at]).astype(jnp.bfloat16)
+    final = pltpu.make_async_copy(end, out.at[pl.ds(early, QUERY_BLOCK)], sems.at[1])
+    final.start()
+    first.wait()
+    final.wait()
+
+
+def trig_table(devices, blocks):
     half_dim = HEAD_DIM // 2
     lane = np.arange(LANES)
     frequency = (rope_base ** (-(lane % half_dim) / half_dim)).astype(np.float32)
     sign = np.where(lane % HEAD_DIM < half_dim, -1.0, 1.0)
     near = np.arange(QUERY_BLOCK)[:, None] * frequency.astype(np.float64)
     far = (np.arange(blocks)[:, None] * np.float32(QUERY_BLOCK) * frequency).astype(np.float64)
-    parts = [np.cos(near), sign * np.sin(near), np.cos(far), sign * np.sin(far)]
-    return np.concatenate(parts, axis=0).astype(np.float32)
+    near = np.concatenate([np.cos(near), sign * np.sin(near)], axis=0)
+    far = np.stack([np.cos(far), sign * np.sin(far)]).reshape(2, devices, -1, LANES)
+    far = far.transpose(1, 0, 2, 3).reshape(devices, -1, LANES)
+    return near.astype(np.float32), far.astype(np.float32)
 
 
 def body(
@@ -483,23 +510,30 @@
     bf16, f32 = jnp.bfloat16, jnp.float32
     slots = chosen_owner.shape[1:][::-1]
     key_count = devices * KEY_BLOCK + QUERY_BLOCK
-    trig = trig_table(devices * qblocks)
+    near_trig, far_trig = trig_table(devices, devices * qblocks)
     operands = [
         chosen_owner[0].T, chosen_part[0].T, row_data, query_weight, key_weight, value_weight,
-        out_weight, norm_gain[None], jnp.asarray(trig),
+        out_weight, norm_gain[None], jnp.asarray(near_trig), jnp.asarray(far_trig),
     ]
     operands = [pltpu.with_memory_space_constraint(x, pltpu.HBM) for x in operands]
     result = pl.pallas_call(
         functools.partial(kernel, devices),
-        out_shape=pltpu.VMEM((count, half), bf16),
+        out_shape=[
+            pltpu.VMEM((count, half), bf16),
+            pltpu.VMEM((QUERY_BLOCK, heads_width), bf16),
+            pltpu.VMEM(out_weight.shape, bf16),
+            pltpu.VMEM((QUERY_BLOCK, 2 * half), bf16),
+            pltpu.VMEM((1, half), f32),
+        ],
         in_specs=[hbm] * len(operands),
-        out_specs=vmem,
+        out_specs=[vmem] * 5,
         scratch_shapes=[
             pltpu.SMEM(slots, jnp.int32),
             pltpu.SMEM(slots, jnp.int32),
             pltpu.VMEM((1, half), f32),
-            pltpu.VMEM(trig.shape, f32),
-            pltpu.SemaphoreType.DMA((4,)),
+            pltpu.VMEM(near_trig.shape, f32),
+            pltpu.VMEM(far_trig.shape[1:], f32),
+            pltpu.SemaphoreType.DMA((5,)),
             pltpu.VMEM((count, LANES), f32),
             pltpu.VMEM((count, LANES), f32),
             pltpu.VMEM((QUERY_BLOCK, QUERY_BLOCK), bf16),
@@ -520,8 +554,7 @@
             pltpu.VMEM((heads_width // LANES * QUERY_BLOCK, 2 * key_count), bf16),
             pltpu.VMEM((count, heads_width), bf16),
             pltpu.VMEM((count, heads_width), bf16),
-            pltpu.VMEM(out_weight.shape, bf16),
-            pltpu.VMEM((QUERY_BLOCK, 2 * half), bf16),
+            pltpu.VMEM((QUERY_BLOCK, half), bf16),
             pltpu.VMEM((count, half), f32),
             pltpu.VMEM((qblocks, QUERY_BLOCK, LANES), f32),
             pltpu.VMEM((qblocks, QUERY_BLOCK, LANES), f32),
@@ -537,14 +570,19 @@
             collective_id=0, has_side_effects=True, vmem_limit_bytes=48 * 1024 * 1024
         ),
     )(*operands)
+    result = [pltpu.with_memory_space_constraint(x, pltpu.VMEM) for x in result]
     return pl.pallas_call(
-        store_kernel,
+        finish_kernel,
         out_shape=jax.ShapeDtypeStruct((count, half), bf16),
-        in_specs=[vmem],
+        in_specs=[vmem] * len(result),
         out_specs=hbm,
-        scratch_shapes=[pltpu.SemaphoreType.DMA((qblocks,))],
-        compiler_params=pltpu.CompilerParams(vmem_limit_bytes=4 * 1024 * 1024),
-    )(pltpu.with_memory_space_constraint(result, pltpu.VMEM))[None]
+        scratch_shapes=[
+            pltpu.VMEM((QUERY_BLOCK, half), f32),
+            pltpu.VMEM((QUERY_BLOCK, half), bf16),
+            pltpu.SemaphoreType.DMA((2,)),
+        ],
+        compiler_params=pltpu.CompilerParams(vmem_limit_bytes=8 * 1024 * 1024),
+    )(*result)[None]
 
 
 def solution(mesh):

time: 25.7 us -> 25.4 us (0.988)
  Pallas kernels: 25.5 us -> 25.2 us
    pallas_call x2, Pallas kernels: 25.5 us -> 25.2 us  [the longest x1 23.7 us: body(): pl.pallas_call(functools.partial(kernel, devices), out_shape=[pltpu.VMEM(...]
where the time goes in v5:
time: 25.4 us; the launch traced here: 25.2 us
  Pallas kernels  25.2 us (99%)
    pallas_call x1, Pallas kernels, body(): pl.pallas_call(functools.partial(kernel, devices), out_shape=[pltpu.VMEM(...  23.7 us
    pallas_call x1, Pallas kernels, body(): pl.pallas_call(finish_kernel, out_shape=jax.ShapeDtypeStruct((count, half...  1.47 us

profile of v5, /device:TPU:23, one launch (start us, length us, event | category | flops | bytes accessed | tf_op | source)
XLA Modules:
  0.0 25.2 jit_solution(761427765049680368)
XLA Ops:
  0.0 23.7 %shard_map.100 = (bf16[768,1024]{1,0:T(8,128)(2,1)S(1)}, bf16[128,512]{1,0:T(8,128)(2,1)S(1)}, bf16[512,2048]{1,0:T(8,128)(2,1)S(1)}, bf16[128,2048]{1,0:T(8,128)(2,1)S(1)}, f32[1,1024]{1,0:T(1,128)S(1)}) custom-call(s32[4,24]{1,0:T(4,128)} %bitcast.11, s32[4,24]{1,0:T(4,128)} %bitcast.12, bf16[768,2048]{1,0:T(8,128)(2,1)} %bitcast.9, ...), custom_call_target="tpu_custom_call" | custom-call | tf_op jit(solution)/shard_map/pallas_call | solution.py:519
  23.8 1.5 %shard_map.101 = bf16[768,1024]{1,0:T(8,128)(2,1)} custom-call(bf16[768,1024]{1,0:T(8,128)(2,1)S(1)} %get-tuple-element.10.held, bf16[128,512]{1,0:T(8,128)(2,1)S(1)} %get-tuple-element.11.mix_end, bf16[512,2048]{1,0:T(8,128)(2,1)S(1)} %get-tuple-element.12.ow_other, bf16[128,2048]{1,0:T(8,128)(2,1)S(1)} %get-tuple-element.13.partial, ...), custom_call_target="tpu_custom_call" | custom-call | tf_op jit(solution)/shard_map/pallas_call | solution.py:574

commit v6 on v5

--- a/solution.py
+++ b/solution.py
@@ -196,10 +196,8 @@
 
         if split:
 
-            @pl.loop(0, devices - 1)
-            def _(step):
-                dst = devices - 1 - step
-
+            @pl.loop(1, devices)
+            def _(dst):
                 @pl.when(dst > me)
                 def _():
                     kv_copy(dst, q, value_lanes, qblocks).start()
@@ -361,19 +359,35 @@
             device_id_type=MESH,
         )
 
-    def project_mine(first):
-        rows = pl.ds(pl.multiple_of(first * QUERY_BLOCK, QUERY_BLOCK), QUERY_BLOCK)
-        for c in range(half // COLS):
-            early[:, c * COLS : (c + 1) * COLS] = part_of(mix, ow, rows, half, core, c)
-
-    def project(first, count, ready=False):
+    def project_mine(first, held):
+        rows = pl.ds(first * QUERY_BLOCK, QUERY_BLOCK)
+        for n, side in enumerate((other, core)):
+            for c in range(half // COLS):
+                at = n * half + c * COLS
+                held[:, at : at + COLS] = part_of(mix, ow, rows, half, side, c)
+
+    def project_whole(first):
+        wait_mix(first, 1)
+        rows = pl.ds(first * QUERY_BLOCK, QUERY_BLOCK)
+        total = jnp.zeros((QUERY_BLOCK, LANES), f32)
+        for n, side in enumerate((other, core)):
+            for c in range(half // COLS):
+                at = n * half + c * COLS
+                theirs = part_of(mix_other, ow_other, rows, half, side, c)
+                added = early[:, at : at + COLS].astype(f32) + theirs.astype(f32)
+                if side is core:
+                    proj[rows, c * COLS : (c + 1) * COLS] = added
+                total = squares(total, added)
+        normed(rows, total)
+
+    def project(first, count):
         wait_mix(first, count)
         size = count * QUERY_BLOCK
         rows = pl.ds(pl.multiple_of(first * QUERY_BLOCK, QUERY_BLOCK), size)
         total = jnp.zeros((size, LANES), f32)
         for c in range(half // COLS):
             at = slice(c * COLS, (c + 1) * COLS)
-            mine = early[:, at] if ready else part_of(mix, ow, rows, half, core, c)
+            mine = part_of(mix, ow, rows, half, core, c)
             theirs = part_of(mix_other, ow_other, rows, half, core, c)
             added = mine.astype(f32) + theirs.astype(f32)
             proj[rows, at] = added
@@ -392,11 +406,10 @@
         landed = ss_other.at[pl.ds(first, count)]
         pltpu.make_async_copy(landed, landed, ss_recv.at[group_of(first)]).wait()
 
-        @pl.loop(0, count)
-        def _(j):
-            b = first + j
-            rows = pl.ds(pl.multiple_of(b * QUERY_BLOCK, QUERY_BLOCK), QUERY_BLOCK)
-            normed(rows, ss[b] + ss_other[b])
+        size = count * QUERY_BLOCK
+        rows = pl.ds(pl.multiple_of(first * QUERY_BLOCK, QUERY_BLOCK), size)
+        blocks = pl.ds(first, count)
+        normed(rows, (ss[blocks] + ss_other[blocks]).reshape(size, LANES))
 
     @pl.loop(0, last)
     def _(b):
@@ -428,18 +441,14 @@
     def _():
         send_block(last, True)
 
-    project_mine(last - 1)
+    project_mine(last - 1, early)
     gain_end[...] = gain[...]
     wait_kv(last, key_lanes, last)
     attend_keys(last)
     wait_kv(last, value_lanes, qblocks)
     attend_values(last)
-    project(last - 1, 1, ready=True)
-    final = slice(last * QUERY_BLOCK, qblocks * QUERY_BLOCK)
-    for n, side in enumerate((other, core)):
-        for c in range(half // COLS):
-            at = n * half + c * COLS
-            partial[:, at : at + COLS] = part_of(mix, ow, final, half, side, c)
+    project_mine(last, partial)
+    project_whole(last - 1)
 
     @pl.loop(0, devices)
     def _(dst):
@@ -449,10 +458,10 @@
             pltpu.make_async_copy(sent, sent, kv_send.at[dst]).wait()
 
     ow_copy.wait_send()
-    pltpu.make_async_copy(ss.at[pl.ds(0, last)], ss.at[pl.ds(0, last)], ss_send.at[0]).wait()
+    shared = ss.at[pl.ds(0, last - 1)]
+    pltpu.make_async_copy(shared, shared, ss_send.at[0]).wait()
     pltpu.make_async_copy(mix_end, mix_end, mix_recv.at[group_of(last)]).wait()
     pltpu.make_async_copy(mix, mix, mix_send.at[0]).wait()
-    norm(last - 1, 1)
 
 
 def finish_kernel(held, mix_end, ow_other, partial, gain, out, proj, end, sems):
@@ -554,17 +563,17 @@
             pltpu.VMEM((heads_width // LANES * QUERY_BLOCK, 2 * key_count), bf16),
             pltpu.VMEM((count, heads_width), bf16),
             pltpu.VMEM((count, heads_width), bf16),
-            pltpu.VMEM((QUERY_BLOCK, half), bf16),
+            pltpu.VMEM((QUERY_BLOCK, 2 * half), bf16),
             pltpu.VMEM((count, half), f32),
-            pltpu.VMEM((qblocks, QUERY_BLOCK, LANES), f32),
-            pltpu.VMEM((qblocks, QUERY_BLOCK, LANES), f32),
+            pltpu.VMEM((qblocks - 2, QUERY_BLOCK, LANES), f32),
+            pltpu.VMEM((qblocks - 2, QUERY_BLOCK, LANES), f32),
             pltpu.SemaphoreType.DMA((devices,)),
             pltpu.SemaphoreType.DMA((qblocks + 1,)),
             pltpu.SemaphoreType.DMA((2,)),
             pltpu.SemaphoreType.DMA((1,)),
             pltpu.SemaphoreType.DMA((count // ROWS + 1,)),
             pltpu.SemaphoreType.DMA((1,)),
-            pltpu.SemaphoreType.DMA((count // ROWS,)),
+            pltpu.SemaphoreType.DMA((count // ROWS - 1,)),
         ],
         compiler_params=pltpu.CompilerParams(
             collective_id=0, has_side_effects=True, vmem_limit_bytes=48 * 1024 * 1024

time: 25.4 us -> 25 us (0.984)
  Pallas kernels: 25.2 us -> 24.8 us
    pallas_call x1, Pallas kernels: 23.7 us -> 23.3 us  [body(): pl.pallas_call(functools.partial(kernel, devices), out_shape=[pltpu.VMEM(...]
where the time goes in v6:
time: 25 us; the launch traced here: 24.8 us
  Pallas kernels  24.8 us (99%)
    pallas_call x1, Pallas kernels, body(): pl.pallas_call(functools.partial(kernel, devices), out_shape=[pltpu.VMEM(...  23.3 us
    pallas_call x1, Pallas kernels, body(): pl.pallas_call(finish_kernel, out_shape=jax.ShapeDtypeStruct((count, half...  1.46 us

profile of v6, /device:TPU:23, one launch (start us, length us, event | category | flops | bytes accessed | tf_op | source)
XLA Modules:
  0.0 24.8 jit_solution(549643599715867379)
XLA Ops:
  0.0 23.3 %shard_map.100 = (bf16[768,1024]{1,0:T(8,128)(2,1)S(1)}, bf16[128,512]{1,0:T(8,128)(2,1)S(1)}, bf16[512,2048]{1,0:T(8,128)(2,1)S(1)}, bf16[128,2048]{1,0:T(8,128)(2,1)S(1)}, f32[1,1024]{1,0:T(1,128)S(1)}) custom-call(s32[4,24]{1,0:T(4,128)} %bitcast.11, s32[4,24]{1,0:T(4,128)} %bitcast.12, bf16[768,2048]{1,0:T(8,128)(2,1)} %bitcast.9, ...), custom_call_target="tpu_custom_call" | custom-call | tf_op jit(solution)/shard_map/pallas_call | solution.py:528
  23.4 1.5 %shard_map.101 = bf16[768,1024]{1,0:T(8,128)(2,1)} custom-call(bf16[768,1024]{1,0:T(8,128)(2,1)S(1)} %get-tuple-element.10.held, bf16[128,512]{1,0:T(8,128)(2,1)S(1)} %get-tuple-element.11.mix_end, bf16[512,2048]{1,0:T(8,128)(2,1)S(1)} %get-tuple-element.12.ow_other, bf16[128,2048]{1,0:T(8,128)(2,1)S(1)} %get-tuple-element.13.partial, ...), custom_call_target="tpu_custom_call" | custom-call | tf_op jit(solution)/shard_map/pallas_call | solution.py:583

commit v7 on v6

--- a/solution.py
+++ b/solution.py
@@ -56,8 +56,8 @@
     devices, owner_hbm, part_hbm, tok_hbm, wq_hbm, wk_hbm, wv_hbm, ow_hbm, gain_hbm, near_hbm, far_hbm, out, mix_end, ow_other, partial, gain_end,
     owner_ref, part_ref, gain, near_trig, far_trig, small_sems, cosine, sine, eye, causal,
     tok, wq, wkv, ow, tok_sems, weight_sems,
-    kv, send, pool, queries, keys_now, values_now, scores, weights, mix, mix_other, early, proj, ss, ss_other,
-    kv_send, kv_recv, ow_sems, mix_send, mix_recv, ss_send, ss_recv,
+    kv, send, pool, queries, keys_now, values_now, scores, weights, mix, mix_other, early, proj,
+    kv_send, kv_recv, ow_sems, mix_send, mix_recv,
 ):
     me = lax.axis_index("kv")
     core = lax.axis_index("tp")
@@ -173,7 +173,7 @@
         return pltpu.make_async_remote_copy(
             src_ref=send.at[pl.ds(dst * qblocks + q, 1), :, lanes],
             dst_ref=pool.at[pl.ds(q * devices + me, 1), :, lanes],
-            send_sem=kv_send.at[dst],
+            send_sem=kv_send.at[0],
             recv_sem=kv_recv.at[sem],
             device_id={"kv": dst},
             device_id_type=MESH,
@@ -184,10 +184,12 @@
         pl.ds(0, 2 * LANES), pl.ds(0, LANES), pl.ds(LANES, LANES)
     )
 
+    paced = me + 3 < devices
+
     def send_block(q, split):
         @pl.loop(0, devices - 1)
         def _(step):
-            dst = devices - 1 - step
+            dst = jnp.where(paced, step + 1, devices - 1 - step)
 
             @pl.when(dst > me)
             def _():
@@ -201,8 +203,6 @@
                 @pl.when(dst > me)
                 def _():
                     kv_copy(dst, q, value_lanes, qblocks).start()
-
-    paced = me + 3 < devices
 
     @pl.loop(0, jnp.where(paced, 1, last))
     def _(q):
@@ -349,67 +349,31 @@
             )
         mix_copy(b).start()
 
-    def ss_copy(b):
-        return pltpu.make_async_remote_copy(
-            src_ref=ss.at[b],
-            dst_ref=ss_other.at[b],
-            send_sem=ss_send.at[0],
-            recv_sem=ss_recv.at[group_of(b)],
-            device_id={"tp": other},
-            device_id_type=MESH,
-        )
-
-    def project_mine(first, held):
-        rows = pl.ds(first * QUERY_BLOCK, QUERY_BLOCK)
+    def project_mine(first, count, held):
+        size = count * QUERY_BLOCK
+        rows = pl.ds(pl.multiple_of(first * QUERY_BLOCK, QUERY_BLOCK), size)
         for n, side in enumerate((other, core)):
             for c in range(half // COLS):
                 at = n * half + c * COLS
-                held[:, at : at + COLS] = part_of(mix, ow, rows, half, side, c)
-
-    def project_whole(first):
-        wait_mix(first, 1)
-        rows = pl.ds(first * QUERY_BLOCK, QUERY_BLOCK)
-        total = jnp.zeros((QUERY_BLOCK, LANES), f32)
+                held[:size, at : at + COLS] = part_of(mix, ow, rows, half, side, c)
+
+    def project_theirs(first, count):
+        wait_mix(first, count)
+        size = count * QUERY_BLOCK
+        rows = pl.ds(pl.multiple_of(first * QUERY_BLOCK, QUERY_BLOCK), size)
+        total = jnp.zeros((size, LANES), f32)
         for n, side in enumerate((other, core)):
             for c in range(half // COLS):
                 at = n * half + c * COLS
                 theirs = part_of(mix_other, ow_other, rows, half, side, c)
-                added = early[:, at : at + COLS].astype(f32) + theirs.astype(f32)
+                added = early[:size, at : at + COLS].astype(f32) + theirs.astype(f32)
                 if side is core:
-                    proj[rows, c * COLS : (c + 1) * COLS] = added
+                    proj[:size, c * COLS : (c + 1) * COLS] = added
                 total = squares(total, added)
-        normed(rows, total)
-
-    def project(first, count):
-        wait_mix(first, count)
-        size = count * QUERY_BLOCK
-        rows = pl.ds(pl.multiple_of(first * QUERY_BLOCK, QUERY_BLOCK), size)
-        total = jnp.zeros((size, LANES), f32)
-        for c in range(half // COLS):
-            at = slice(c * COLS, (c + 1) * COLS)
-            mine = part_of(mix, ow, rows, half, core, c)
-            theirs = part_of(mix_other, ow_other, rows, half, core, c)
-            added = mine.astype(f32) + theirs.astype(f32)
-            proj[rows, at] = added
-            total = squares(total, added)
-        for j in range(count):
-            ss[first + j] = total[j * QUERY_BLOCK : (j + 1) * QUERY_BLOCK]
-            ss_copy(first + j).start()
-
-    def normed(rows, total):
         scale = row_scale(total, half)
         for c in range(half // LANES):
             at = slice(c * LANES, (c + 1) * LANES)
-            out[rows, at] = (proj[rows, at] * scale * gain[:, at]).astype(bf16)
-
-    def norm(first, count):
-        landed = ss_other.at[pl.ds(first, count)]
-        pltpu.make_async_copy(landed, landed, ss_recv.at[group_of(first)]).wait()
-
-        size = count * QUERY_BLOCK
-        rows = pl.ds(pl.multiple_of(first * QUERY_BLOCK, QUERY_BLOCK), size)
-        blocks = pl.ds(first, count)
-        normed(rows, (ss[blocks] + ss_other[blocks]).reshape(size, LANES))
+            out[rows, at] = (proj[:size, at] * scale * gain[:, at]).astype(bf16)
 
     @pl.loop(0, last)
     def _(b):
@@ -427,39 +391,34 @@
 
         @pl.when(b % blocks_in == blocks_in - 1)
         def _():
-            project(b + 1 - blocks_in, blocks_in)
+            project_mine(b + 1 - blocks_in, blocks_in, early)
+            project_theirs(b + 1 - blocks_in, blocks_in)
 
         @pl.when(jnp.logical_and(paced, b == last - 2))
         def _():
             send_block(last - 1, False)
-
-        @pl.when(jnp.logical_and(b > 0, b % blocks_in == 0))
-        def _():
-            norm(b - blocks_in, blocks_in)
 
     @pl.when(paced)
     def _():
         send_block(last, True)
 
-    project_mine(last - 1, early)
+    project_mine(last - 1, 1, early)
     gain_end[...] = gain[...]
     wait_kv(last, key_lanes, last)
     attend_keys(last)
     wait_kv(last, value_lanes, qblocks)
     attend_values(last)
-    project_mine(last, partial)
-    project_whole(last - 1)
-
-    @pl.loop(0, devices)
-    def _(dst):
-        @pl.when(dst > me)
-        def _():
-            sent = send.at[pl.ds(dst * qblocks, qblocks)]
-            pltpu.make_async_copy(sent, sent, kv_send.at[dst]).wait()
+    project_mine(last, 1, partial)
+    project_theirs(last - 1, 1)
+
+    for n in range(devices - 1):
+
+        @pl.when(me == n)
+        def _():
+            sent = send.at[pl.ds((n + 1) * qblocks, (devices - 1 - n) * qblocks)]
+            pltpu.make_async_copy(sent, sent, kv_send.at[0]).wait()
 
     ow_copy.wait_send()
-    shared = ss.at[pl.ds(0, last - 1)]
-    pltpu.make_async_copy(shared, shared, ss_send.at[0]).wait()
     pltpu.make_async_copy(mix_end, mix_end, mix_recv.at[group_of(last)]).wait()
     pltpu.make_async_copy(mix, mix, mix_send.at[0]).wait()
 
@@ -563,17 +522,13 @@
             pltpu.VMEM((heads_width // LANES * QUERY_BLOCK, 2 * key_count), bf16),
             pltpu.VMEM((count, heads_width), bf16),
             pltpu.VMEM((count, heads_width), bf16),
-            pltpu.VMEM((QUERY_BLOCK, 2 * half), bf16),
-            pltpu.VMEM((count, half), f32),
-            pltpu.VMEM((qblocks - 2, QUERY_BLOCK, LANES), f32),
-            pltpu.VMEM((qblocks - 2, QUERY_BLOCK, LANES), f32),
-            pltpu.SemaphoreType.DMA((devices,)),
+            pltpu.VMEM((ROWS, 2 * half), bf16),
+            pltpu.VMEM((ROWS, half), f32),
+            pltpu.SemaphoreType.DMA((1,)),
             pltpu.SemaphoreType.DMA((qblocks + 1,)),
             pltpu.SemaphoreType.DMA((2,)),
             pltpu.SemaphoreType.DMA((1,)),
             pltpu.SemaphoreType.DMA((count // ROWS + 1,)),
-            pltpu.SemaphoreType.DMA((1,)),
-            pltpu.SemaphoreType.DMA((count // ROWS - 1,)),
         ],
         compiler_params=pltpu.CompilerParams(
             collective_id=0, has_side_effects=True, vmem_limit_bytes=48 * 1024 * 1024

time: 25 us -> 25.9 us (1.036)
  Pallas kernels: 24.8 us -> 25.7 us
    pallas_call x1, Pallas kernels: 23.3 us -> 24.3 us  [body(): pl.pallas_call(functools.partial(kernel, devices), out_shape=[pltpu.VMEM(...]
where the time goes in v7:
time: 25.9 us; the launch traced here: 25.7 us
  Pallas kernels  25.7 us (99%)
    pallas_call x1, Pallas kernels, body(): pl.pallas_call(functools.partial(kernel, devices), out_shape=[pltpu.VMEM(...  24.3 us
    pallas_call x1, Pallas kernels, body(): pl.pallas_call(finish_kernel, out_shape=jax.ShapeDtypeStruct((count, half...  1.46 us

profile of v7, /device:TPU:23, one launch (start us, length us, event | category | flops | bytes accessed | tf_op | source)
XLA Modules:
  0.0 25.7 jit_solution(14735250312128153271)
XLA Ops:
  0.0 24.3 %shard_map.100 = (bf16[768,1024]{1,0:T(8,128)(2,1)S(1)}, bf16[128,512]{1,0:T(8,128)(2,1)S(1)}, bf16[512,2048]{1,0:T(8,128)(2,1)S(1)}, bf16[128,2048]{1,0:T(8,128)(2,1)S(1)}, f32[1,1024]{1,0:T(1,128)S(1)}) custom-call(s32[4,24]{1,0:T(4,128)} %bitcast.11, s32[4,24]{1,0:T(4,128)} %bitcast.12, bf16[768,2048]{1,0:T(8,128)(2,1)} %bitcast.9, ...), custom_call_target="tpu_custom_call" | custom-call | tf_op jit(solution)/shard_map/pallas_call | solution.py:487
  24.3 1.5 %shard_map.101 = bf16[768,1024]{1,0:T(8,128)(2,1)} custom-call(bf16[768,1024]{1,0:T(8,128)(2,1)S(1)} %get-tuple-element.10.held, bf16[128,512]{1,0:T(8,128)(2,1)S(1)} %get-tuple-element.11.mix_end, bf16[512,2048]{1,0:T(8,128)(2,1)S(1)} %get-tuple-element.12.ow_other, bf16[128,2048]{1,0:T(8,128)(2,1)S(1)} %get-tuple-element.13.partial, ...), custom_call_target="tpu_custom_call" | custom-call | tf_op jit(solution)/shard_map/pallas_call | solution.py:538

commit v8 on v7

--- a/solution.py
+++ b/solution.py
@@ -73,7 +73,8 @@
     heads = wq.shape[1] // HEAD_DIM
     bf16, f32 = jnp.bfloat16, jnp.float32
 
-    pieces = ((0, ROWS), (ROWS, tokens - ROWS))
+    first_rows = tokens // KEY_BLOCK * 5 // 12 * KEY_BLOCK
+    pieces = ((0, first_rows), (first_rows, tokens - first_rows))
 
     def tok_copy(r):
         rows = pl.ds(*pieces[r])
@@ -189,7 +190,7 @@
     def send_block(q, split):
         @pl.loop(0, devices - 1)
         def _(step):
-            dst = jnp.where(paced, step + 1, devices - 1 - step)
+            dst = devices - 1 - step
 
             @pl.when(dst > me)
             def _():

time: 25.9 us -> 24.9 us (0.961)
  Pallas kernels: 25.7 us -> 24.8 us
    pallas_call x1, Pallas kernels: 24.3 us -> 23.3 us  [body(): pl.pallas_call(functools.partial(kernel, devices), out_shape=[pltpu.VMEM(...]
where the time goes in v8:
time: 24.9 us; the launch traced here: 24.8 us
  Pallas kernels  24.8 us (100%)
    pallas_call x1, Pallas kernels, body(): pl.pallas_call(functools.partial(kernel, devices), out_shape=[pltpu.VMEM(...  23.3 us
    pallas_call x1, Pallas kernels, body(): pl.pallas_call(finish_kernel, out_shape=jax.ShapeDtypeStruct((count, half...  1.46 us

profile of v8, /device:TPU:23, one launch (start us, length us, event | category | flops | bytes accessed | tf_op | source)
XLA Modules:
  0.0 24.8 jit_solution(5498718061289982231)
XLA Ops:
  0.0 23.3 %shard_map.100 = (bf16[768,1024]{1,0:T(8,128)(2,1)S(1)}, bf16[128,512]{1,0:T(8,128)(2,1)S(1)}, bf16[512,2048]{1,0:T(8,128)(2,1)S(1)}, bf16[128,2048]{1,0:T(8,128)(2,1)S(1)}, f32[1,1024]{1,0:T(1,128)S(1)}) custom-call(s32[4,24]{1,0:T(4,128)} %bitcast.11, s32[4,24]{1,0:T(4,128)} %bitcast.12, bf16[768,2048]{1,0:T(8,128)(2,1)} %bitcast.9, ...), custom_call_target="tpu_custom_call" | custom-call | tf_op jit(solution)/shard_map/pallas_call | solution.py:488
  23.3 1.5 %shard_map.101 = bf16[768,1024]{1,0:T(8,128)(2,1)} custom-call(bf16[768,1024]{1,0:T(8,128)(2,1)S(1)} %get-tuple-element.10.held, bf16[128,512]{1,0:T(8,128)(2,1)S(1)} %get-tuple-element.11.mix_end, bf16[512,2048]{1,0:T(8,128)(2,1)S(1)} %get-tuple-element.12.ow_other, bf16[128,2048]{1,0:T(8,128)(2,1)S(1)} %get-tuple-element.13.partial, ...), custom_call_target="tpu_custom_call" | custom-call | tf_op jit(solution)/shard_map/pallas_call | solution.py:539
